TPU v7x, 32 devices: a whole 2x2x4 slice. The times are simulated.
32 devices in a mesh: ep: 8 (over z, y), tp: 4 (over x, core).
Axes of the slice: x: 2, y: 2, z: 4, core: 2. Of those that a mesh axis runs over, the one named last changes fastest.
Arguments:
- tokens_a: bfloat16 [1024, 2048], P('ep'), may hold values from -30 to 30
- attn_gain: float32 [2048], replicated, may hold values from 0.1 to 1.9
- w_query: bfloat16 [2048, 2048], P(None, 'tp'), may hold values from -2 to 2
- w_query_rot: bfloat16 [2048, 1024], P(None, 'tp'), may hold values from -0.125 to 0.125
- w_latent: bfloat16 [2048, 512], replicated, may hold values from -2 to 2
- w_key_rot: bfloat16 [2048, 32], replicated, may hold values from -0.125 to 0.125
- latent_gain: float32 [512], replicated, may hold values from 0.1 to 1.9
- w_key_up: bfloat16 [512, 2048], P(None, 'tp'), may hold values from -2 to 2
- w_value_up: bfloat16 [512, 2048], P(None, 'tp'), may hold values from -0.25 to 0.25
- w_output: bfloat16 [2048, 2048], P('tp'), may hold values from -0.125 to 0.125
- tokens_b: bfloat16 [2048, 2048], P('ep'), may hold values from -6 to 6
- ffn_gain: float32 [2048], replicated, may hold values from 0.1 to 1.9
- expert_ids: int32 [2048, 2], P('ep'), may hold values from 0 to 7, all different within a row; in each aligned block of 256 rows (0 to 255, 256 to 511, ...) at most 128 rows name the same one
- expert_weights: float32 [2048, 2], P('ep'), may hold values from 0.1 to 1
- w_gate: bfloat16 [8, 2048, 1024], P('ep', None, 'tp'), may hold values from -0.125 to 0.125
- w_up: bfloat16 [8, 2048, 1024], P('ep', None, 'tp'), may hold values from -0.125 to 0.125
- w_down: bfloat16 [8, 1024, 2048], P('ep', 'tp'), may hold values from -0.1875 to 0.1875
Outputs:
- mixed_a: bfloat16 [1024, 2048], P(('ep', 'tp'))
- mixed_b: bfloat16 [2048, 2048], P('ep', 'tp')
Inputs may be any that keep to these rules, and one draw needn't show every extreme that they name: `expert_ids`: each row names 2 different experts. In the 256 rows of one index of ep no expert is named more than 128 times, and in some such block one expert is named exactly 128 times.
All inputs are finite; a program needn't handle non-finite values.
Results may differ from a plain program's by a relative error of at most 0.012.
Values may be sent and summed in bfloat16 or wider, within the bound.
A program may use at most 192 MiB of HBM per device.

v0:
```python
import jax
import jax.numpy as jnp
from jax import lax
from jax.sharding import PartitionSpec as P

NOPE = 64
ROPE = 32
VD = 64


epsilon = 1e-06
rope_base = 10000.0


def normalize(matrix, gain):
    floats = matrix.astype(jnp.float32)
    scaled = floats * lax.rsqrt(jnp.mean(floats * floats, axis=-1, keepdims=True) + epsilon)
    return scaled * gain


def rotate(vectors, positions):
    rot_width = vectors.shape[-1]
    half_width = rot_width // 2
    inverse = rope_base ** (-(jnp.arange(half_width, dtype=jnp.float32) * 2.0) / rot_width)
    angles = positions.astype(jnp.float32)[:, None] * inverse[None, :]
    cosine = jnp.cos(angles)[:, None, :]
    sine_part = jnp.sin(angles)[:, None, :]
    first_half = vectors[..., :half_width]
    second_half = vectors[..., half_width:]
    return jnp.concatenate(
        [
            first_half * cosine - second_half * sine_part,
            first_half * sine_part + second_half * cosine,
        ],
        axis=-1,
    )


def attention_half(
    tokens_a,
    attn_gain,
    w_query,
    w_query_rot,
    w_latent,
    w_key_rot,
    latent_gain,
    w_key_up,
    w_value_up,
    w_output,
    outgoing,
):
    row_count = tokens_a.shape[0]
    head_count = w_query.shape[1] // NOPE
    offset = lax.axis_index("ep") * row_count
    positions = offset + jnp.arange(row_count, dtype=jnp.int32)
    normed = normalize(tokens_a, attn_gain).astype(jnp.bfloat16)
    query_plain = jnp.dot(normed, w_query, preferred_element_type=jnp.float32).astype(jnp.bfloat16)
    query_plain = query_plain.reshape(row_count, head_count, NOPE)
    turned = jnp.dot(normed, w_query_rot, preferred_element_type=jnp.float32).reshape(
        row_count, head_count, ROPE
    )
    query_rotated_rows = rotate(turned, positions).astype(jnp.bfloat16)
    latent = normalize(
        jnp.dot(normed, w_latent, preferred_element_type=jnp.float32), latent_gain
    ).astype(jnp.bfloat16)
    key_raw = jnp.dot(normed, w_key_rot, preferred_element_type=jnp.float32)[:, None, :]
    key_turned = rotate(key_raw, positions)[:, 0, :].astype(jnp.bfloat16)
    logit_scale = (NOPE + ROPE) ** (-0.5)
    outgoing, compact = lax.optimization_barrier(
        (outgoing, jnp.concatenate([latent, key_turned], axis=1))
    )
    joined = lax.all_gather(compact, "ep", axis=0, tiled=True)
    arrived = lax.all_to_all(outgoing, "ep", split_axis=0, concat_axis=0, tiled=True)
    pieces = (joined[:, : latent.shape[1]], joined[:, latent.shape[1] :])
    piece_keys = jnp.dot(pieces[0], w_key_up, preferred_element_type=jnp.float32).astype(
        jnp.bfloat16
    )
    piece_values = jnp.dot(pieces[0], w_value_up, preferred_element_type=jnp.float32).astype(
        jnp.bfloat16
    )
    key_count = piece_keys.shape[0]
    blocks = key_count // row_count
    key_blocks = piece_keys.reshape(blocks, row_count, head_count, NOPE)
    value_blocks = piece_values.reshape(blocks, row_count, head_count, VD)
    rotated_key_blocks = pieces[1].reshape(blocks, row_count, ROPE)
    score_matrix = (
        jnp.einsum("yvz,wrvz->yvwr", query_plain, key_blocks, preferred_element_type=jnp.float32)
        + jnp.einsum(
            "yjx,inx->yjin",
            query_rotated_rows,
            rotated_key_blocks,
            preferred_element_type=jnp.float32,
        )
    ) * logit_scale
    key_pos = jnp.arange(key_count, dtype=jnp.int32).reshape(blocks, row_count)
    allowed = key_pos[None, None, :, :] <= positions[:, None, None, None]
    masked = jnp.where(allowed, score_matrix, -1e30)
    block_max = jnp.max(masked, axis=-1)
    probs = jnp.where(allowed, jnp.exp(masked - block_max[..., None]), 0.0)
    block_total = jnp.sum(probs, axis=-1)
    block_out = jnp.einsum(
        "qhbk,bkhd->qhbd",
        probs.astype(jnp.bfloat16),
        value_blocks,
        preferred_element_type=jnp.float32,
    )
    run_max = jnp.full((row_count, head_count), -1e30, jnp.float32)
    new_max = jnp.maximum(run_max, jnp.max(block_max, axis=-1))
    new_factor = jnp.exp(block_max - new_max[..., None])
    new_total = jnp.sum(new_factor * block_total, axis=-1)
    new_out = jnp.sum(new_factor[..., None] * block_out, axis=2)
    attended = (
        (new_out / new_total[..., None]).astype(jnp.bfloat16).reshape(row_count, head_count * VD)
    )
    mixed = lax.psum_scatter(
        jnp.dot(attended, w_output, preferred_element_type=jnp.float32).astype(jnp.bfloat16),
        "tp",
        scatter_dimension=0,
        tiled=True,
    )
    return mixed, arrived


def dispatch_rows(tokens_b, ffn_gain, expert_ids, expert_count):
    row_count, width = tokens_b.shape
    top_count = expert_ids.shape[1]
    capacity = 2 * row_count * top_count // expert_count
    tp_count = lax.axis_size("tp")
    part_width = width // tp_count
    floats = tokens_b.astype(jnp.float32)
    factor = lax.rsqrt(jnp.mean(floats * floats, axis=-1, keepdims=True) + epsilon)
    start = lax.axis_index("tp") * part_width
    own = lax.dynamic_slice_in_dim(tokens_b, start, part_width, 1).astype(jnp.float32)
    own_gain = lax.dynamic_slice_in_dim(ffn_gain, start, part_width, 0)
    normed = (own * factor * own_gain).astype(jnp.bfloat16)
    experts = jnp.arange(expert_count, dtype=jnp.int32)
    slots = jnp.arange(capacity, dtype=jnp.int32)
    named = (expert_ids[:, :, None] == experts).any(axis=1)
    rows = jnp.arange(row_count, dtype=jnp.int32)
    earlier = (rows[:, None] > rows[None, :]).astype(jnp.bfloat16)
    before = jnp.dot(
        earlier, named.astype(jnp.bfloat16), preferred_element_type=jnp.float32
    ).astype(jnp.int32)
    slot_of = jnp.where(named, before, -1).T
    chosen = (slot_of[:, None, :] == slots[None, :, None]).astype(jnp.bfloat16)
    outgoing = jnp.dot(
        chosen.reshape(expert_count * capacity, row_count),
        normed,
        preferred_element_type=jnp.float32,
    ).astype(jnp.bfloat16)
    outgoing = outgoing.reshape(expert_count, capacity, part_width)
    return outgoing, before


def swap(block, distance, count):
    return lax.ppermute(block, "tp", [(i, i ^ distance) for i in range(count)])


def expert_half(arrived, before, expert_ids, expert_weights, w_gate, w_up, w_down):
    expert_count, capacity, part_width = arrived.shape
    tp_count = lax.axis_size("tp")
    top_count = expert_ids.shape[1]
    experts = jnp.arange(expert_count, dtype=jnp.int32)
    me = lax.axis_index("tp")
    blocks = {0: arrived.reshape(-1, part_width)}
    distance = tp_count // 2
    while distance:
        for mask in list(blocks):
            blocks[mask ^ distance] = swap(blocks[mask], distance, tp_count)
        distance //= 2
    gate_part = 0.0
    up_part = 0.0
    for mask, block in blocks.items():
        first = (me ^ mask) * part_width
        gate_rows = lax.dynamic_slice_in_dim(w_gate[0], first, part_width, 0)
        up_rows = lax.dynamic_slice_in_dim(w_up[0], first, part_width, 0)
        gate_part += jnp.dot(block, gate_rows, preferred_element_type=jnp.float32)
        up_part += jnp.dot(block, up_rows, preferred_element_type=jnp.float32)
    hidden = (jax.nn.silu(gate_part) * up_part).astype(jnp.bfloat16)
    parts = {}
    for mask in reversed(range(tp_count)):
        down_columns = lax.dynamic_slice_in_dim(w_down[0], (me ^ mask) * part_width, part_width, 1)
        parts[mask] = jnp.dot(hidden, down_columns, preferred_element_type=jnp.float32)
    distance = 1
    while distance < tp_count:
        for mask in [m for m in parts if m & distance]:
            came = swap(parts.pop(mask).astype(jnp.bfloat16), distance, tp_count)
            parts[mask ^ distance] += came.astype(jnp.float32)
        distance *= 2
    summed = parts[0].astype(jnp.bfloat16)
    returned = lax.all_to_all(
        summed.reshape(expert_count, capacity, part_width),
        "ep",
        split_axis=0,
        concat_axis=0,
        tiled=True,
    )
    shares = expert_weights / jnp.sum(expert_weights, axis=1, keepdims=True)
    table = returned.reshape(expert_count * capacity, part_width)
    total = 0.0
    for k in range(top_count):
        own_slot = jnp.sum(jnp.where(expert_ids[:, k : k + 1] == experts, before, 0), axis=1)
        target = expert_ids[:, k] * capacity + own_slot
        pick = (
            target[:, None] == jnp.arange(expert_count * capacity, dtype=jnp.int32)
        ).astype(jnp.bfloat16)
        picked = jnp.dot(pick, table, preferred_element_type=jnp.float32)
        total = total + picked * shares[:, k : k + 1]
    return total.astype(jnp.bfloat16)


def on_device(
    tokens_a,
    attn_gain,
    w_query,
    w_query_rot,
    w_latent,
    w_key_rot,
    latent_gain,
    w_key_up,
    w_value_up,
    w_output,
    tokens_b,
    ffn_gain,
    expert_ids,
    expert_weights,
    w_gate,
    w_up,
    w_down,
):
    expert_count = w_gate.shape[0] * lax.axis_size("ep")
    outgoing, before = dispatch_rows(tokens_b, ffn_gain, expert_ids, expert_count)
    mixed_a, arrived = attention_half(
        tokens_a,
        attn_gain,
        w_query,
        w_query_rot,
        w_latent,
        w_key_rot,
        latent_gain,
        w_key_up,
        w_value_up,
        w_output,
        outgoing,
    )
    mixed_b = expert_half(arrived, before, expert_ids, expert_weights, w_gate, w_up, w_down)
    return (mixed_a, mixed_b)


def solution(mesh):
    placed = (
        P("ep", None),
        P(),
        P(None, "tp"),
        P(None, "tp"),
        P(),
        P(),
        P(),
        P(None, "tp"),
        P(None, "tp"),
        P("tp", None),
        P("ep", None),
        P(),
        P("ep", None),
        P("ep", None),
        P("ep", None, "tp"),
        P("ep", None, "tp"),
        P("ep", "tp", None),
    )
    return jax.shard_map(
        on_device,
        mesh=mesh,
        in_specs=placed,
        out_specs=(P(("ep", "tp"), None), P("ep", "tp")),
        check_vma=False,
    )
```

profile of v0, /device:TPU:0, one launch (start us, length us, event | category | flops | bytes accessed | tf_op | source)
XLA Modules:
  0.0 170.8 jit_solution(8710696470042588831)
XLA Ops:
  7.2 0.9 fusion.95
  8.1 0.7 fusion.63
  8.8 1.5 multiply_reduce_fusion
  10.3 1.2 fusion.15
  11.6 1.4 convolution_bitcast_fusion
  13.3 2.2 %multiply_reduce_fusion.1 = (f32[128]{0:T(128)S(1)}, f32[128,512]{1,0:T(8,128)S(1)}) fusion(bf16[2048,512]{1,0:T(8,128)(2,1)} %param.21, bf16[128,2048]{1,0:T(8,128)(2,1)S(1)} %copy-done.7, f32[2048]{0:T(1024)S(1)} %copy-done.12, f32[128]{0:T(128)S(1)} %add_rsqrt_fusion.2), kind=kOutput, calls=%fused_computation.81 | convolution fusion | flops 269614976 | bytes 2892800 | tf_op jit(solution)/shard_map/dot_general | solution.py:64
  15.4 0.8 dynamic_slice.67
  16.7 0.7 pad_maximum_fusion
  17.4 2.5 %convolution_convert_fusion.1 = bf16[1024,512]{1,0:T(8,128)(2,1)} fusion(pred[1024,256]{1,0:T(32,128)(4,1)S(1)} %bitcast_compare_fusion, f32[512]{0:T(512)S(1)} %dynamic_slice.67, f32[256]{0:T(256)S(1)} %add_rsqrt_fusion, bf16[256,2048]{1,0:T(8,128)(2,1)} %param.27, s32[]{:T(128)S(6)} %select_n.45), kind=kOutput, calls=%fused_computation.19 | convolution fusion | flops 269484032 | bytes 1575940 | tf_op jit(solution)/shard_map/dot_general | solution.py:146
  19.9 7.3 %all-to-all-start = ((bf16[8,128,512]{2,1,0:T(8,128)(2,1)}), bf16[8,128,512]{2,1,0:T(8,128)(2,1)S(1)}, u32[]{:S(2)}, u32[]{:S(2)}) async-start(bf16[8,128,512]{2,1,0:T(8,128)(2,1)} %bitcast.118), calls=%async_computation.1 | async-start | bytes 2097152 | tf_op jit(solution)/shard_map/all_to_all | solution.py:73
  27.2 0.7 all-gather.2.cloned.1.call-update
  28.0 2.3 %convolution_convert_fusion.6 = bf16[128,512]{1,0:T(8,128)(2,1)S(1)} fusion(bf16[2048,512]{1,0:T(8,128)(2,1)} %param.19, bf16[128,2048]{1,0:T(8,128)(2,1)} %param.17, f32[2048]{0:T(1024)S(1)} %copy-done.12, f32[128]{0:T(128)S(1)} %add_rsqrt_fusion.2), kind=kOutput, calls=%fused_computation.36 | convolution fusion | flops 269549568 | bytes 2761216 | tf_op jit(solution)/shard_map/dot_general | solution.py:57
  30.5 2.0 %fusion.88 = f32[128,256]{0,1:T(8,128)S(1)} fusion(bf16[2048,256]{1,0:T(8,128)(2,1)} %param.20, bf16[128,2048]{1,0:T(8,128)(2,1)} %param.17, f32[2048]{0:T(1024)S(1)} %copy-done.12, f32[128]{0:T(128)S(1)} %add_rsqrt_fusion.2), kind=kOutput, calls=%fused_computation.142 | convolution fusion | flops 135266304 | bytes 1712640 | tf_op jit(solution)/shard_map/dot_general | solution.py:59
  32.5 25.7 %all-to-all-done = bf16[8,128,512]{2,1,0:T(8,128)(2,1)S(1)} async-done(((bf16[8,128,512]{2,1,0:T(8,128)(2,1)}), bf16[8,128,512]{2,1,0:T(8,128)(2,1)S(1)}, u32[]{:S(2)}, u32[]{:S(2)}) %all-to-all-start) | async-done | bytes 1048608 | tf_op jit(solution)/shard_map/all_to_all | solution.py:73
  58.2 1.5 collective-permute-start
  60.0 2.4 %fusion.44 = f32[1024,256]{1,0:T(8,128)} fusion(bf16[1024,512]{1,0:T(8,128)(2,1)S(1)} %bitcast.116, bf16[1,2048,256]{2,1,0:T(8,128)(2,1)} %param.31, s32[]{:T(128)S(6)} %select_n.45), kind=kOutput, calls=%fused_computation.65 | convolution fusion | flops 268435456 | bytes 2359300 | tf_op jit(solution)/shard_map/dot_general | solution.py:177
  62.4 2.4 %fusion.39 = f32[1024,256]{1,0:T(8,128)} fusion(bf16[1024,512]{1,0:T(8,128)(2,1)S(1)} %bitcast.117, bf16[1,2048,256]{2,1,0:T(8,128)(2,1)} %param.32, s32[]{:T(128)S(6)} %select_n.45), kind=kOutput, calls=%fused_computation.60 | convolution fusion | flops 268435456 | bytes 2359300 | tf_op jit(solution)/shard_map/dot_general | solution.py:178
  64.8 14.4 %all-gather.2.cloned.1.call-done = bf16[1024,544]{1,0:T(8,128)(2,1)} async-done(((bf16[128,544]{1,0:T(8,128)(2,1)}), bf16[1024,544]{1,0:T(8,128)(2,1)}) %all-gather.2.cloned.1.call-update) | async-done | bytes 1114128 | tf_op jit(solution)/shard_map/all_gather | solution.py:72
  79.2 3.1 %convolution_convert_fusion.5 = bf16[1024,512]{1,0:T(8,128)(2,1)} fusion(bf16[512,512]{1,0:T(8,128)(2,1)} %param.24, bf16[1024,544]{1,0:T(8,128)(2,1)} %all-gather.2.cloned.1.call-done), kind=kOutput, calls=%fused_computation.23 | convolution fusion | flops 537395200 | bytes 2621440 | tf_op jit(solution)/shard_map/dot_general | solution.py:75
  82.3 3.9 %reshape.230 = bf16[8,128,8,64]{3,2,1,0:T(8,128)(2,1)} reshape(bf16[1024,512]{1,0:T(8,128)(2,1)} %convolution_convert_fusion.5) | data formatting | bytes 2097152 | tf_op jit(solution)/shard_map/reshape | solution.py:83
  86.3 2.2 %convolution_add_fusion.5 = f32[1024,256]{1,0:T(8,128)S(1)} fusion(f32[1024,256]{1,0:T(8,128)} %fusion.44, bf16[1024,512]{1,0:T(8,128)(2,1)} %collective-permute-done, bf16[1,2048,256]{2,1,0:T(8,128)(2,1)} %param.31, s32[]{:T(128)S(6)} %select_n.49), kind=kOutput, calls=%fused_computation.29 | convolution fusion | flops 268697600 | bytes 3407876 | tf_op jit(solution)/shard_map/dot_general | solution.py:177
  88.5 1.7 %convolution_add_fusion.2 = f32[1024,256]{1,0:T(8,128)S(1)} fusion(f32[1024,256]{1,0:T(8,128)S(1)} %copy-done.2, bf16[1024,512]{1,0:T(8,128)(2,1)} %collective-permute-done, bf16[1,2048,256]{2,1,0:T(8,128)(2,1)S(1)} %copy-done.6, s32[]{:T(128)S(6)} %select_n.49), kind=kOutput, calls=%fused_computation.26 | convolution fusion | flops 268697600 | bytes 3407876 | tf_op jit(solution)/shard_map/dot_general | solution.py:178
  90.2 1.7 convolution_add_fusion.4
  91.9 1.7 convolution_add_fusion.1
  93.6 0.4 convolution_add_fusion.3
  94.1 0.4 multiply_convert_fusion
  94.5 0.8 copy-done.5
  95.3 0.4 convolution_convert_fusion.2
  95.7 0.4 collective-permute-start.4
  96.2 0.7 fusion.8
  96.8 0.3 slice-done
  97.1 2.9 %fusion.96 = (f32[128,8,8]{0,2,1:T(8,128)S(1)}, f32[128,8,8,128]{0,3,2,1:T(8,128)}) fusion(bf16[8,128,32,1]{2,1,0,3:T(8,128)(2,1)S(1)} %bitcast.119, bf16[128,8,16]{0,2,1:T(8,128)(2,1)S(1)} %get-tuple-element.13, bf16[128,8,16]{0,2,1:T(8,128)(2,1)S(1)} %get-tuple-element.12, f32[8,8,128,128]{3,2,1,0:T(8,128)S(1)} %fusion.8, ...), kind=kOutput, calls=%fused_computation.146 | convolution fusion | flops 71426048 | bytes 8683520 | tf_op jit(solution)/shard_map/yjx,inx->yjin/dot_general | solution.py:88
  100.0 1.5 convolution_convert_fusion.3
  101.7 1.4 add_convert_fusion.1
  103.1 1.5 collective-permute-start.5
  104.6 1.7 convolution_convert_fusion.4
  106.3 3.9 %reshape.231 = bf16[8,128,8,64]{3,2,1,0:T(8,128)(2,1)} reshape(bf16[1024,512]{1,0:T(8,128)(2,1)} %convolution_convert_fusion.4) | data formatting | bytes 2097152 | tf_op jit(solution)/shard_map/reshape | solution.py:84
  110.2 3.2 %fusion.2 = (f32[128,8,8]{0,2,1:T(8,128)S(1)}, f32[128,8]{0,1:T(8,128)S(1)}) fusion(f32[128,8,8,128]{0,3,2,1:T(8,128)} %get-tuple-element.28, f32[128,8,8]{0,2,1:T(8,128)S(1)} %get-tuple-element.27, pred[128,8,128]{0,2,1:T(8,128)(4,1)S(1)} %broadcast_compare_fusion), kind=kLoop, calls=%fused_computation.4 | loop fusion | flops 4185088 | bytes 4395008 | tf_op jit(solution)/shard_map/reduce_sum | solution.py:100
  113.4 1.4 fusion.32
  114.8 14.0 %collective-permute-done.5 = bf16[1024,512]{1,0:T(8,128)(2,1)} collective-permute-done((bf16[1024,512]{1,0:T(8,128)(2,1)}, bf16[1024,512]{1,0:T(8,128)(2,1)}, u32[]{:S(2)}, u32[]{:S(2)}) %collective-permute-start.5) | collective-permute-done | bytes 1048608 | tf_op jit(solution)/shard_map/ppermute | solution.py:156
  128.8 3.0 %add_convert_fusion = bf16[1024,512]{1,0:T(8,128)(2,1)} fusion(bf16[1024,512]{1,0:T(8,128)(2,1)} %collective-permute-done.5, f32[1024,512]{1,0:T(8,128)S(1)} %fusion.32, bf16[1024,512]{1,0:T(8,128)(2,1)} %collective-permute-done.3), kind=kLoop, calls=%fused_computation.13 | loop fusion | flops 2621440 | bytes 5242880 | tf_op jit(solution)/shard_map/convert_element_type | solution.py:190
  131.9 3.7 %all-to-all-start.1 = ((bf16[8,128,512]{2,1,0:T(8,128)(2,1)}), bf16[8,128,512]{2,1,0:T(8,128)(2,1)S(1)}, u32[]{:S(2)}, u32[]{:S(2)}) async-start(bf16[8,128,512]{2,1,0:T(8,128)(2,1)} %bitcast.33), calls=%async_computation.2 | async-start | bytes 2097152 | tf_op jit(solution)/shard_map/all_to_all | solution.py:191
  135.7 4.0 %fusion.6 = f32[128,8,64]{0,2,1:T(8,128)S(1)} fusion(f32[128,8,8]{0,2,1:T(8,128)S(1)} %get-tuple-element.11, f32[128,8,8,128]{0,3,2,1:T(8,128)} %get-tuple-element.28, f32[128,8,8]{0,2,1:T(8,128)S(1)} %get-tuple-element.27, pred[128,8,128]{0,2,1:T(8,128)(4,1)S(1)} %broadcast_compare_fusion, bf16[8,128,8,64]{3,2,1,0:T(8,128)(2,1)} %reshape.231), kind=kOutput, calls=%fused_computation.9 | convolution fusion | flops 138346496 | bytes 5701632 | tf_op jit(solution)/shard_map/qhbk,bkhd->qhbd/dot_general | solution.py:101
  139.7 1.3 convolution_convert_fusion
  141.1 19.9 %all-to-all-done.1 = bf16[8,128,512]{2,1,0:T(8,128)(2,1)S(1)} async-done(((bf16[8,128,512]{2,1,0:T(8,128)(2,1)}), bf16[8,128,512]{2,1,0:T(8,128)(2,1)S(1)}, u32[]{:S(2)}, u32[]{:S(2)}) %all-to-all-start.1) | async-done | bytes 1048608 | tf_op jit(solution)/shard_map/all_to_all | solution.py:191
  161.0 0.5 convolution_multiply_fusion
  161.5 1.2 fusion.14
  162.7 1.2 reduce-scatter.2.cloned.1.call-done
  (62 shorter events, 1.9 us)
Async XLA Ops:
  7.2 132.5 %copy-start = (bf16[512,2048]{1,0:T(8,128)(2,1)S(1)}, bf16[512,2048]{1,0:T(8,128)(2,1)}, u32[]{:S(2)}) copy-start(bf16[512,2048]{1,0:T(8,128)(2,1)} %param.26) | copy-start | bytes 6291460
  7.2 6.1 %copy-start.7 = (bf16[128,2048]{1,0:T(8,128)(2,1)S(1)}, bf16[128,2048]{1,0:T(8,128)(2,1)}, u32[]{:S(2)}) copy-start(bf16[128,2048]{1,0:T(8,128)(2,1)} %param.17) | copy-start | bytes 1572868
  7.2 6.1 %copy-start.12 = (f32[2048]{0:T(1024)S(1)}, f32[2048]{0:T(1024)}, u32[]{:S(2)}) copy-start(f32[2048]{0:T(1024)} %param.18) | copy-start | bytes 24580
  11.5 5.1 %copy-start.10 = (f32[512]{0:T(512)S(1)}, f32[512]{0:T(512)}, u32[]{:S(2)}) copy-start(f32[512]{0:T(512)} %param.23) | copy-start | bytes 6148
  19.9 38.3 %all-to-all-start = ((bf16[8,128,512]{2,1,0:T(8,128)(2,1)}), bf16[8,128,512]{2,1,0:T(8,128)(2,1)S(1)}, u32[]{:S(2)}, u32[]{:S(2)}) async-start(bf16[8,128,512]{2,1,0:T(8,128)(2,1)} %bitcast.118), calls=%async_computation.1 | async-start | bytes 2097152 | tf_op jit(solution)/shard_map/all_to_all | solution.py:73
  27.2 3.2 %copy-start.9 = (f32[256,2]{0,1:T(2,128)S(1)}, f32[256,2]{0,1:T(2,128)}, u32[]{:S(2)}) copy-start(f32[256,2]{0,1:T(2,128)} %param.30) | copy-start | bytes 6148
  27.2 52.0 %all-gather.2.cloned.1.call-start = ((), (), s32[]{:S(2)}) async-start(), calls=%async_computation.3 | async-start | bytes 1474560 | tf_op jit(solution)/shard_map/all_gather | solution.py:72
  58.2 27.9 %collective-permute-start = (bf16[1024,512]{1,0:T(8,128)(2,1)S(1)}, bf16[1024,512]{1,0:T(8,128)(2,1)}, u32[]{:S(2)}, u32[]{:S(2)}) collective-permute-start(bf16[1024,512]{1,0:T(8,128)(2,1)S(1)} %bitcast.114), channel_id=1, source_target_pairs={{0,2},{1,3},{2,0},{3,1},{4,6},{5,7},{6,4},{7,5},{8,10},{9,11},{10,... | collective-permute-start | bytes 3145736 | tf_op jit(solution)/shard_map/ppermute | solution.py:156
  59.9 30.3 %collective-permute-start.1 = (bf16[1024,512]{1,0:T(8,128)(2,1)S(1)}, bf16[1024,512]{1,0:T(8,128)(2,1)}, u32[]{:S(2)}, u32[]{:S(2)}) collective-permute-start(bf16[1024,512]{1,0:T(8,128)(2,1)S(1)} %bitcast.115), channel_id=1, source_target_pairs={{0,1},{1,0},{2,3},{3,2},{4,5},{5,4},{6,7},{7,6},{8,9},{9,8},{10,11... | collective-permute-start | bytes 3145736 | tf_op jit(solution)/shard_map/ppermute | solution.py:156
  86.2 2.3 %copy-start.2 = (f32[1024,256]{1,0:T(8,128)S(1)}, f32[1024,256]{1,0:T(8,128)}, u32[]{:S(2)}) copy-start(f32[1024,256]{1,0:T(8,128)} %fusion.39) | copy-start | bytes 3145732
  86.2 2.3 %copy-start.6 = (bf16[1,2048,256]{2,1,0:T(8,128)(2,1)S(1)}, bf16[1,2048,256]{2,1,0:T(8,128)(2,1)}, u32[]{:S(2)}) copy-start(bf16[1,2048,256]{2,1,0:T(8,128)(2,1)} %param.32) | copy-start | bytes 3145732
  86.2 7.4 %collective-permute-start.2 = (bf16[1024,512]{1,0:T(8,128)(2,1)}, bf16[1024,512]{1,0:T(8,128)(2,1)S(1)}, u32[]{:S(2)}, u32[]{:S(2)}) collective-permute-start(bf16[1024,512]{1,0:T(8,128)(2,1)} %collective-permute-done), channel_id=1, source_target_pairs={{0,1},{1,0},{2,3},{3,2},{4,5},{5,4},{6,7},{7,6},{8,9},{9,8},{10,11... | collective-permute-start | bytes 3145736 | tf_op jit(solution)/shard_map/ppermute | solution.py:156
  88.5 1.8 %copy-start.3 = (bf16[1,2048,256]{2,1,0:T(8,128)(2,1)S(1)}, bf16[1,2048,256]{2,1,0:T(8,128)(2,1)}, u32[]{:S(2)}) copy-start(bf16[1,2048,256]{2,1,0:T(8,128)(2,1)} %param.31) | copy-start | bytes 3145732
  94.1 1.2 copy-start.5
  94.1 2.1 %copy-start.1 = (bf16[8,128,8,64]{3,2,1,0:T(8,128)(2,1)S(1)}, bf16[8,128,8,64]{3,2,1,0:T(8,128)(2,1)}, u32[]{:S(2)}) copy-start(bf16[8,128,8,64]{3,2,1,0:T(8,128)(2,1)} %reshape.230) | copy-start | bytes 3145732
  95.7 6.0 %collective-permute-start.4 = (bf16[1024,512]{1,0:T(8,128)(2,1)S(1)}, bf16[1024,512]{1,0:T(8,128)(2,1)S(1)}, u32[]{:S(2)}, u32[]{:S(2)}) collective-permute-start(bf16[1024,512]{1,0:T(8,128)(2,1)S(1)} %convolution_convert_fusion.2), channel_id=1, source_target_pairs={{0,1},{1,0},{2,3},{3,2},{4,5},{5,4},{6,7},{7,6},{8,9},{9,8},{10,11... | collective-permute-start | bytes 3145736 | tf_op jit(solution)/shard_map/ppermute | solution.py:156
  96.2 1.0 slice-start
  100.0 4.6 %copy-start.4 = (bf16[1024,544]{1,0:T(8,128)(2,1)S(1)}, bf16[1024,544]{1,0:T(8,128)(2,1)}, u32[]{:S(2)}) copy-start(bf16[1024,544]{1,0:T(8,128)(2,1)} %all-gather.2.cloned.1.call-done) | copy-start | bytes 3342340
  100.0 4.6 %copy-start.11 = (bf16[512,512]{1,0:T(8,128)(2,1)S(1)}, bf16[512,512]{1,0:T(8,128)(2,1)}, u32[]{:S(2)}) copy-start(bf16[512,512]{1,0:T(8,128)(2,1)} %param.25) | copy-start | bytes 1572868
  101.5 13.3 %collective-permute-start.3 = (bf16[1024,512]{1,0:T(8,128)(2,1)}, bf16[1024,512]{1,0:T(8,128)(2,1)}, u32[]{:S(2)}, u32[]{:S(2)}) collective-permute-start(bf16[1024,512]{1,0:T(8,128)(2,1)} %convolution_convert_fusion.3), channel_id=1, source_target_pairs={{0,1},{1,0},{2,3},{3,2},{4,5},{5,4},{6,7},{7,6},{8,9},{9,8},{10,11... | collective-permute-start | bytes 3145736 | tf_op jit(solution)/shard_map/ppermute | solution.py:156
  103.1 25.7 %collective-permute-start.5 = (bf16[1024,512]{1,0:T(8,128)(2,1)}, bf16[1024,512]{1,0:T(8,128)(2,1)}, u32[]{:S(2)}, u32[]{:S(2)}) collective-permute-start(bf16[1024,512]{1,0:T(8,128)(2,1)} %add_convert_fusion.1), channel_id=1, source_target_pairs={{0,2},{1,3},{2,0},{3,1},{4,6},{5,7},{6,4},{7,5},{8,10},{9,11},{10,... | collective-permute-start | bytes 3145736 | tf_op jit(solution)/shard_map/ppermute | solution.py:156
  131.9 29.1 %all-to-all-start.1 = ((bf16[8,128,512]{2,1,0:T(8,128)(2,1)}), bf16[8,128,512]{2,1,0:T(8,128)(2,1)S(1)}, u32[]{:S(2)}, u32[]{:S(2)}) async-start(bf16[8,128,512]{2,1,0:T(8,128)(2,1)} %bitcast.33), calls=%async_computation.2 | async-start | bytes 2097152 | tf_op jit(solution)/shard_map/all_to_all | solution.py:191
  135.6 28.3 %reduce-scatter.2.cloned.1.call-start = ((), (), s32[]{:S(2)}) async-start(), calls=%async_computation.4 | async-start | bytes 655360 | tf_op jit(solution)/shard_map/reduce_scatter | solution.py:115
  139.7 1.4 copy-start.8
Sparse Core Ops, SparseCore 0:
  30.8 48.3 all-gather.1
  141.1 22.7 reduce-scatter.1
where the time goes:
time: 172 us; the launch traced here: 171 us
  waiting for transfers between devices  76 us (44%)
  matrix products  43.4 us (25%)
  starting transfers between devices  14.9 us (9%)
  between operations  14.5 us (8%)
  other arithmetic  11.3 us (7%)
  local copies, waits for them, and re-layouts  10.7 us (6%)
    all_to_all x1, waiting for transfers between devices, attention_half(): lax.all_to_all(outgoing, 'ep', split_axis=0, concat_axis=0, tiled=True)  25.7 us
    all_to_all x1, waiting for transfers between devices, expert_half(): lax.all_to_all(summed.reshape(expert_count, capacity, part_width), 'ep',...  19.9 us
    all_gather x1, waiting for transfers between devices, attention_half(): joined = lax.all_gather(compact, 'ep', axis=0, tiled=True)  14.4 us
    ppermute x6, waiting for transfers between devices, swap(): return lax.ppermute(block, 'tp', [(i, i ^ distance) for i in range(count)])  14 us
    all_to_all x1, starting transfers between devices, attention_half(): lax.all_to_all(outgoing, 'ep', split_axis=0, concat_axis=0, tiled=True)  7.31 us
    dot_general x4, matrix products, expert_half(): gate_part += jnp.dot(block, gate_rows, preferred_element_type=jnp.float32)  6.69 us
    dot_general x4, matrix products, expert_half(): up_part += jnp.dot(block, up_rows, preferred_element_type=jnp.float32)  6.22 us
    dot_general x4, matrix products, expert_half(): jnp.dot(hidden, down_columns, preferred_element_type=jnp.float32)  4.71 us
  transfers between devices with their start and end apart: 10, of which 5 were waited for; matrix products, arithmetic and copies ran while one was open for 28% of the time, Pallas kernels for 0%

commit v1 on v0

--- a/solution.py
+++ b/solution.py
@@ -1,11 +1,20 @@
+import dataclasses
+import functools
+import math
+
 import jax
 import jax.numpy as jnp
+import numpy as np
 from jax import lax
+from jax.experimental import pallas as pl
+from jax.experimental.pallas import tpu as pltpu
 from jax.sharding import PartitionSpec as P
 
 NOPE = 64
 ROPE = 32
 VD = 64
+LANES = 128
+VMEM_BYTES = 60 * 1024 * 1024
 
 
 epsilon = 1e-06
@@ -209,6 +218,536 @@
     return total.astype(jnp.bfloat16)
 
 
+def rope_tables(rows, blocks):
+    half = ROPE // 2
+    lane = np.arange(LANES) % ROPE
+    inverse = rope_base ** (-((lane % half).astype(np.float64) * 2.0) / ROPE)
+    near = np.arange(rows, dtype=np.float64)[:, None] * inverse[None, :]
+    far = (np.arange(blocks, dtype=np.float64) * rows)[:, None] * inverse[None, :]
+    pack = lambda v: np.asarray(v, np.float32)
+    return pack(np.stack([np.cos(near), np.sin(near)])), pack(
+        np.stack([np.cos(far), np.sin(far)], axis=1)
+    )
+
+
+def fused_kernel(
+    dims,
+    ta_hbm, ag_ref, wq_hbm, wqr_hbm, wl_hbm, wkr_hbm, lg_ref, wku_hbm, wvu_hbm, wo_hbm,
+    tb_hbm, fg_ref, ids_ref, wts_ref, wg_hbm, wu_hbm, wd_hbm, near_ref, far_ref,
+    out_a, out_b,
+    ta, wq, wqr, wl, wkr, wku, wvu, wo, tb, wg, wu, wd,
+    own_b, slot_t, slot_c, share_c, staged, landed, part_keep, part_send, part_recv,
+    pair_send, pair_recv, back_send, back_recv, total,
+    normed_a, rot_w, lat, qs, keys, vals, att, mixed, am_send, am_recv, ax_send, ax_recv,
+    load_sem, z_send, z_recv, x_send, x_recv, c_send, c_recv, f_send, f_recv,
+    p_send, p_recv, q_send, q_recv, b_send, b_recv,
+    lz_send, lz_recv, ly_send, ly_recv, ld_send, ld_recv, as_send, as_recv, at_send, at_recv,
+):
+    n, cap, rows_a, rows_b = dims.n, dims.cap, dims.rows_a, dims.rows_b
+    width = dims.width
+    e, t = lax.axis_index("ep"), lax.axis_index("tp")
+    core = lax.rem(t, 2)
+    mate, across = t + 1 - 2 * core, lax.rem(t + 2, 4)
+    third = lax.rem(mate + 2, 4)
+    quarter = (t, mate, across, third)
+    beside = e + 1 - 2 * lax.rem(e, 2)
+
+    def plus(k):
+        return lax.rem(e + k, n)
+
+    def minus(k):
+        return lax.rem(e + n - k, n)
+
+    def remote(src, dst, ssem, rsem, ep=None, tp=None):
+        target = (e if ep is None else ep, t if tp is None else tp)
+        return pltpu.make_async_remote_copy(
+            src_ref=src, dst_ref=dst, send_sem=ssem, recv_sem=rsem,
+            device_id=target, device_id_type=pl.DeviceIdType.MESH,
+        )
+
+    pairs = [
+        (tb_hbm, tb), (ta_hbm, ta), (wl_hbm, wl), (wkr_hbm, wkr), (wg_hbm, wg), (wu_hbm, wu),
+        (wd_hbm, wd), (wq_hbm, wq), (wqr_hbm, wqr), (wku_hbm, wku), (wvu_hbm, wvu), (wo_hbm, wo),
+    ]
+    loads = [pltpu.make_async_copy(s, d, load_sem.at[i]) for i, (s, d) in enumerate(pairs)]
+    for load in loads:
+        load.start()
+    (l_tb, l_ta, l_wl, l_wkr, l_wg, l_wu, l_wd, l_wq, l_wqr, l_wku, l_wvu, l_wo) = loads
+
+    barrier = pltpu.get_barrier_semaphore()
+    for k in range(1, n):
+        pl.semaphore_signal(
+            barrier, inc=1, device_id=(plus(k), t), device_id_type=pl.DeviceIdType.MESH
+        )
+    for peer in (mate, across):
+        pl.semaphore_signal(
+            barrier, inc=1, device_id=(e, peer), device_id_type=pl.DeviceIdType.MESH
+        )
+
+    def own_columns(which):
+        return pl.ds(pl.multiple_of(which * width, width), width)
+
+    ids = ids_ref[...]
+    sub = lax.broadcasted_iota(jnp.int32, (LANES, rows_b), 0)
+    first, second = ids[0:1] == sub, ids[1:2] == sub
+    named = jnp.logical_or(first, second)
+    earlier = (
+        lax.broadcasted_iota(jnp.int32, (rows_b, rows_b), 0)
+        < lax.broadcasted_iota(jnp.int32, (rows_b, rows_b), 1)
+    ).astype(jnp.float32).astype(jnp.bfloat16)
+    before = jnp.dot(
+        named.astype(jnp.float32).astype(jnp.bfloat16), earlier, preferred_element_type=jnp.float32
+    )
+    slot = jnp.where(named, before, -1.0)
+    slot_t[...] = slot
+    slot_c[...] = slot.T
+    weight = wts_ref[...]
+    sum_weight = weight[0:1] + weight[1:2]
+    share_c[...] = (
+        jnp.where(first, weight[0:1] / sum_weight, 0.0)
+        + jnp.where(second, weight[1:2] / sum_weight, 0.0)
+    ).T
+
+    l_tb.wait()
+    floats = tb[...].astype(jnp.float32)
+    factor = lax.rsqrt(jnp.mean(floats * floats, axis=-1, keepdims=True) + epsilon)
+    columns = own_columns(t)
+    own_b[...] = (
+        tb[:, columns].astype(jnp.float32) * factor * fg_ref[:, columns]
+    ).astype(jnp.bfloat16)
+
+    pl.semaphore_wait(barrier, n + 1)
+
+    def z_copy(m):
+        return remote(staged.at[m], landed.at[0, m], z_send.at[m], z_recv.at[m], ep=plus(m))
+
+    def x_copy(m):
+        return remote(landed.at[0, m], landed.at[2, m], x_send.at[m], x_recv.at[m], tp=across)
+
+    def c_copy(m):
+        return remote(landed.at[0, m], landed.at[1, m], c_send.at[m], c_recv.at[m], tp=mate)
+
+    def f_copy(m):
+        return remote(landed.at[2, m], landed.at[3, m], f_send.at[m], f_recv.at[m], tp=mate)
+
+    def p_copy(m):
+        return remote(part_send.at[m], part_recv.at[m], p_send.at[m], p_recv.at[m], tp=mate)
+
+    def q_copy(m):
+        return remote(pair_send.at[m], pair_recv.at[m], q_send.at[m], q_recv.at[m], tp=across)
+
+    def b_copy(m):
+        return remote(back_send.at[m], back_recv.at[m], b_send.at[m], b_recv.at[m], ep=minus(m))
+
+    def dispatch(m):
+        row = slot_t[pl.ds(plus(m), 1), :]
+        wanted = lax.broadcasted_iota(jnp.int32, (cap, rows_b), 0).astype(jnp.float32)
+        chosen = (row == wanted).astype(jnp.float32).astype(jnp.bfloat16)
+        picked = jnp.dot(chosen, own_b[...], preferred_element_type=jnp.float32)
+        if m:
+            staged[m] = picked.astype(jnp.bfloat16)
+            z_copy(m).start()
+        else:
+            landed[0, 0] = picked.astype(jnp.bfloat16)
+            x_copy(0).start()
+            c_copy(0).start()
+
+    def forward(m):
+        z_copy(m).wait_recv()
+        x_copy(m).start()
+        c_copy(m).start()
+
+    def relay(m):
+        x_copy(m).wait_recv()
+        f_copy(m).start()
+
+    def expert(m):
+        c_copy(m).wait_recv()
+        f_copy(m).wait_recv()
+        gate = up = None
+        for mask in range(4):
+            at = own_columns(quarter[mask])
+            block = landed[mask, m]
+            g = jnp.dot(block, wg[0, at, :], preferred_element_type=jnp.float32)
+            u = jnp.dot(block, wu[0, at, :], preferred_element_type=jnp.float32)
+            gate, up = (g, u) if mask == 0 else (gate + g, up + u)
+        hidden = (gate / (1.0 + jnp.exp(-gate)) * up).astype(jnp.bfloat16)
+        for place, mask in enumerate((1, 3)):
+            part_send[m, place] = jnp.dot(
+                hidden, wd[0, :, own_columns(quarter[mask])], preferred_element_type=jnp.float32
+            ).astype(jnp.bfloat16)
+        p_copy(m).start()
+        for place, mask in enumerate((0, 2)):
+            part_keep[m, place] = jnp.dot(
+                hidden, wd[0, :, own_columns(quarter[mask])], preferred_element_type=jnp.float32
+            )
+
+    def pair_sum(m):
+        p_copy(m).wait_recv()
+        pair_send[m] = (part_keep[m, 1] + part_recv[m, 1].astype(jnp.float32)).astype(jnp.bfloat16)
+        q_copy(m).start()
+        part_keep[m, 0] = part_keep[m, 0] + part_recv[m, 0].astype(jnp.float32)
+
+    def give_back(m):
+        q_copy(m).wait_recv()
+        summed = (part_keep[m, 0] + pair_recv[m].astype(jnp.float32)).astype(jnp.bfloat16)
+        if m:
+            back_send[m] = summed
+            b_copy(m).start()
+        else:
+            back_recv[0] = summed
+
+    def combine(m, begin=False):
+        if m:
+            b_copy(m).wait_recv()
+        expert_at = plus(m)
+        lane = lax.broadcasted_iota(jnp.int32, (rows_b, LANES), 1)
+        here = lane == expert_at
+        at = jnp.sum(jnp.where(here, slot_c[...], 0.0), axis=1, keepdims=True)
+        share = jnp.sum(jnp.where(here, share_c[...], 0.0), axis=1, keepdims=True)
+        wanted = lax.broadcasted_iota(jnp.int32, (rows_b, cap), 1).astype(jnp.float32)
+        pick = (at == wanted).astype(jnp.float32).astype(jnp.bfloat16)
+        picked = jnp.dot(pick, back_recv[m], preferred_element_type=jnp.float32) * share
+        total[...] = picked if begin else total[...] + picked
+
+    half_rows = rows_a // 2
+    mine = pl.ds(pl.multiple_of(core * half_rows, half_rows), half_rows)
+    quads = n // 2
+
+    def lz_copy(k):
+        return remote(
+            lat.at[e, mine], lat.at[e, mine], lz_send.at[k], lz_recv.at[k], ep=plus(2 * k)
+        )
+
+    def lz_arrival(k):
+        block = lat.at[minus(2 * k), mine]
+        return remote(block, block, lz_send.at[k], lz_recv.at[k], ep=plus(2 * k))
+
+    def ly_copy(k):
+        block = lat.at[minus(2 * k), mine]
+        return remote(block, block, ly_send.at[k], ly_recv.at[k], ep=beside)
+
+    def ly_arrival(k):
+        block = lat.at[lax.rem(beside + n - 2 * k, n), mine]
+        return remote(block, block, ly_send.at[k], ly_recv.at[k], ep=beside)
+
+    yours = pl.ds(pl.multiple_of((1 - core) * half_rows, half_rows), half_rows)
+
+    def ld_copy(j, owner, part=None):
+        block = lat.at[owner, mine if part is None else part]
+        return remote(block, block, ld_send.at[j], ld_recv.at[j], tp=mate)
+
+    def owner_of(j):
+        return minus(2 * j) if j < quads else lax.rem(beside + n - 2 * (j - quads), n)
+
+    def latents():
+        l_ta.wait()
+        rows = ta[...].astype(jnp.float32)
+        scale = lax.rsqrt(jnp.mean(rows * rows, axis=-1, keepdims=True) + epsilon)
+        normed_a[...] = (rows * scale * ag_ref[...]).astype(jnp.bfloat16)
+        l_wl.wait()
+        raw = jnp.dot(normed_a[...], wl[...], preferred_element_type=jnp.float32)
+        scale = lax.rsqrt(jnp.mean(raw * raw, axis=-1, keepdims=True) + epsilon)
+        lat[e, :, : dims.rank] = (raw * scale * lg_ref[...]).astype(jnp.bfloat16)
+        l_wkr.wait()
+        plain = wkr[...]
+        swapped = jnp.concatenate([-plain[ROPE // 2 :], plain[: ROPE // 2]], axis=0)
+        for copy in range(LANES // ROPE):
+            rot_w[copy * ROPE : (copy + 1) * ROPE] = plain
+            rot_w[LANES + copy * ROPE : LANES + (copy + 1) * ROPE] = swapped
+        both = lax.dot_general(
+            normed_a[...], rot_w[...], (((1,), (1,)), ((), ())), preferred_element_type=jnp.float32
+        )
+        cosine, sine = turn()
+        lat[e, :, dims.rank :] = (both[:, :LANES] * cosine + both[:, LANES:] * sine).astype(
+            jnp.bfloat16
+        )
+        for k in range(1, quads):
+            lz_copy(k).start()
+        ly_copy(0).start()
+
+    def turn():
+        far = far_ref[e]
+        cosine = near_ref[0] * far[0:1] - near_ref[1] * far[1:2]
+        sine = near_ref[1] * far[0:1] + near_ref[0] * far[1:2]
+        return cosine, sine
+
+    def latents_on():
+        for k in range(1, quads):
+            lz_arrival(k).wait_recv()
+            ly_copy(k).start()
+            ld_copy(k, owner_of(k)).start()
+
+    def latents_over():
+        for k in range(quads):
+            ly_arrival(k).wait_recv()
+            ld_copy(quads + k, owner_of(quads + k)).start()
+
+    def latents_in():
+        for j in range(1, n):
+            ld_copy(j, owner_of(j), yours).wait_recv()
+
+    def queries():
+        l_wq.wait()
+        l_wqr.wait()
+        plain = jnp.dot(normed_a[...], wq[...], preferred_element_type=jnp.float32).astype(
+            jnp.bfloat16
+        )
+        raw = jnp.dot(normed_a[...], wqr[...], preferred_element_type=jnp.float32)
+        cosine, sine = turn()
+        lane = lax.broadcasted_iota(jnp.int32, (rows_a, LANES), 1)
+        low = lax.rem(lane, ROPE) < ROPE // 2
+        turned = []
+        for g in range(raw.shape[1] // LANES):
+            x = raw[:, g * LANES : (g + 1) * LANES]
+            other = jnp.where(
+                low, -pltpu.roll(x, LANES - ROPE // 2, 1), pltpu.roll(x, ROPE // 2, 1)
+            )
+            turned.append(x * cosine + other * sine)
+        for p in range(dims.heads // 2):
+            wide = plain[:, p * LANES : (p + 1) * LANES].astype(jnp.float32)
+            rot = turned[2 * p * ROPE // LANES]
+            for side in range(2):
+                at = (2 * p + side) * ROPE % LANES
+                mine_wide = (lane // NOPE) == side
+                mine_rot = (lane // ROPE) == at // ROPE
+                own = slice(side * rows_a, (side + 1) * rows_a)
+                qs[p, own, :LANES] = jnp.where(mine_wide, wide, 0.0).astype(jnp.bfloat16)
+                qs[p, own, LANES:] = jnp.where(mine_rot, rot, 0.0).astype(jnp.bfloat16)
+
+    def key_values():
+        l_wku.wait()
+        l_wvu.wait()
+        for j in range(n):
+            keys[pl.ds(j * rows_a, rows_a), :] = jnp.dot(
+                lat[j, :, : dims.rank], wku[...], preferred_element_type=jnp.float32
+            ).astype(jnp.bfloat16)
+            vals[pl.ds(j * rows_a, rows_a), :] = jnp.dot(
+                lat[j, :, : dims.rank], wvu[...], preferred_element_type=jnp.float32
+            ).astype(jnp.bfloat16)
+
+    logit_scale = (NOPE + ROPE) ** (-0.5)
+
+    def attend(p):
+        at = slice(p * LANES, (p + 1) * LANES)
+        contract = (((1,), (1,)), ((), ()))
+        scores = []
+        for j in range(n):
+            block = jnp.concatenate(
+                [keys[j * rows_a : (j + 1) * rows_a, at], lat[j, :, dims.rank :]], axis=1
+            )
+            scores.append(
+                lax.dot_general(qs[p], block, contract, preferred_element_type=jnp.float32)
+            )
+        score = jnp.concatenate(scores, axis=1) * logit_scale
+        shape = score.shape
+        position = e * rows_a + lax.rem(lax.broadcasted_iota(jnp.int32, shape, 0), rows_a)
+        allowed = lax.broadcasted_iota(jnp.int32, shape, 1) <= position
+        masked = jnp.where(allowed, score, -1e30)
+        top = jnp.max(masked, axis=1, keepdims=True)
+        probs = jnp.where(allowed, jnp.exp(masked - top), 0.0)
+        weight_sum = jnp.sum(probs, axis=1, keepdims=True)
+        got = jnp.dot(probs.astype(jnp.bfloat16), vals[:, at], preferred_element_type=jnp.float32)
+        got = got / weight_sum
+        lane = lax.broadcasted_iota(jnp.int32, (rows_a, LANES), 1)
+        att[:, at] = jnp.where(lane < VD, got[:rows_a], got[rows_a:]).astype(jnp.bfloat16)
+
+    share_rows = rows_a // 4
+
+    def rows_of(which):
+        return pl.ds(pl.multiple_of(which * share_rows, share_rows), share_rows)
+
+    am_copy = remote(am_send, am_recv, as_send, as_recv, tp=mate)
+    ax_copy = remote(ax_send, ax_recv, at_send, at_recv, tp=across)
+
+    def project():
+        l_wo.wait()
+        mixed[...] = jnp.dot(att[...], wo[...], preferred_element_type=jnp.float32).astype(
+            jnp.bfloat16
+        ).astype(jnp.float32)
+        for place, mask in enumerate((1, 3)):
+            am_send[place] = mixed[rows_of(quarter[mask]), :].astype(jnp.bfloat16)
+        am_copy.start()
+
+    def project_pair():
+        am_copy.wait_recv()
+        ax_send[...] = (mixed[rows_of(across), :] + am_recv[1].astype(jnp.float32)).astype(
+            jnp.bfloat16
+        )
+        ax_copy.start()
+
+    def project_end():
+        ax_copy.wait_recv()
+        out_a[...] = (
+            mixed[rows_of(t), :]
+            + am_recv[0].astype(jnp.float32)
+            + ax_recv[...].astype(jnp.float32)
+        ).astype(jnp.bfloat16)
+
+    dispatch(1)
+    dispatch(0)
+    for m in range(2, n):
+        dispatch(m)
+    latents()
+    l_wg.wait()
+    l_wu.wait()
+    l_wd.wait()
+    order = list(range(1, n)) + [0]
+    pairs_of_heads = dims.heads // 2
+    extra = {0: [queries], 1: [latents_on], 2: [latents_over], 3: [latents_in, key_values]}
+    for p in range(pairs_of_heads):
+        extra.setdefault(4 + p, []).append(functools.partial(attend, p))
+    extra.setdefault(4 + pairs_of_heads, []).append(project)
+    extra.setdefault(5 + pairs_of_heads, []).append(project_pair)
+    for i in range(max(n + 4, 6 + pairs_of_heads)):
+        if i < n - 1:
+            forward(order[i])
+        if i == 0:
+            relay(0)
+        elif i <= n - 1:
+            relay(order[i - 1])
+        if 2 <= i < n + 2:
+            expert(order[i - 2])
+        if 3 <= i < n + 3:
+            pair_sum(order[i - 3])
+        if 4 <= i < n + 4:
+            give_back(order[i - 4])
+        for step in extra.get(i, []):
+            step()
+    for i, m in enumerate(order):
+        combine(m, begin=i == 0)
+    out_b[...] = total[...].astype(jnp.bfloat16)
+    project_end()
+
+    for m in range(n):
+        if m:
+            z_copy(m).wait_send()
+            b_copy(m).wait_send()
+        for make in (x_copy, c_copy, f_copy, p_copy, q_copy):
+            make(m).wait_send()
+    for k in range(quads):
+        if k:
+            lz_copy(k).wait_send()
+        ly_copy(k).wait_send()
+    for j in range(1, n):
+        ld_copy(j, owner_of(j)).wait_send()
+    am_copy.wait_send()
+    ax_copy.wait_send()
+
+
+@dataclasses.dataclass(frozen=True)
+class Dims:
+    n: int
+    cap: int
+    rows_a: int
+    rows_b: int
+    width: int
+    rank: int
+    heads: int
+
+
+def fused_scratch(dims, args):
+    (ta, _, wq, wqr, wl, wkr, _, wku, wvu, wo, tb, _, _, _, wg, wu, wd) = args
+    n, cap, width, rows_a, rows_b = dims.n, dims.cap, dims.width, dims.rows_a, dims.rows_b
+    model = ta.shape[1]
+    bf, f32 = jnp.bfloat16, jnp.float32
+    vmem = pltpu.VMEM
+    copied = [vmem(a.shape, a.dtype) for a in (ta, wq, wqr, wl)]
+    copied.append(vmem((wkr.shape[1], wkr.shape[0]), wkr.dtype))
+    copied += [vmem(a.shape, a.dtype) for a in (wku, wvu, wo, tb, wg, wu, wd)]
+    block = (cap, width)
+    quarter_rows = rows_a // 4
+    return copied, [
+        vmem((rows_b, width), bf),
+        vmem((LANES, rows_b), f32),
+        vmem((rows_b, LANES), f32),
+        vmem((rows_b, LANES), f32),
+        vmem((n, *block), bf),
+        vmem((4, n, *block), bf),
+        vmem((n, 2, *block), f32),
+        vmem((n, 2, *block), bf),
+        vmem((n, 2, *block), bf),
+        vmem((n, *block), bf),
+        vmem((n, *block), bf),
+        vmem((n, *block), bf),
+        vmem((n, *block), bf),
+        vmem((rows_b, width), f32),
+        vmem((rows_a, model), bf),
+        vmem((2 * LANES, model), bf),
+        vmem((n, rows_a, dims.rank + LANES), bf),
+        vmem((dims.heads // 2, 2 * rows_a, 2 * LANES), bf),
+        vmem((n * rows_a, wku.shape[1]), bf),
+        vmem((n * rows_a, wvu.shape[1]), bf),
+        vmem((rows_a, wvu.shape[1]), bf),
+        vmem((rows_a, model), f32),
+        vmem((2, quarter_rows, model), bf),
+        vmem((2, quarter_rows, model), bf),
+        vmem((quarter_rows, model), bf),
+        vmem((quarter_rows, model), bf),
+    ]
+
+
+def fused(dims, args):
+    (ta, ag, wq, wqr, wl, wkr, lg, wku, wvu, wo, tb, fg, ids, wts, wg, wu, wd) = args
+    copied, buffers = fused_scratch(dims, args)
+    n = dims.n
+    dma = pltpu.SemaphoreType.DMA
+    sems = [dma((len(copied),))] + [dma((n,)) for _ in range(14)]
+    sems += [dma((n,)) for _ in range(6)] + [dma, dma, dma, dma]
+    near, far = rope_tables(dims.rows_a, n)
+    anywhere = pl.BlockSpec(memory_space=pl.ANY)
+    inside = pl.BlockSpec(memory_space=pltpu.VMEM)
+    where = [
+        anywhere, inside, anywhere, anywhere, anywhere, anywhere, inside, anywhere, anywhere,
+        anywhere, anywhere, inside, inside, inside, anywhere, anywhere, anywhere, inside, inside,
+    ]
+    return pl.pallas_call(
+        functools.partial(fused_kernel, dims),
+        out_shape=(
+            jax.ShapeDtypeStruct((dims.rows_a // 4, ta.shape[1]), jnp.bfloat16),
+            jax.ShapeDtypeStruct((dims.rows_b, dims.width), jnp.bfloat16),
+        ),
+        in_specs=where,
+        out_specs=(inside, inside),
+        scratch_shapes=copied + buffers + sems,
+        compiler_params=pltpu.CompilerParams(
+            collective_id=0, has_side_effects=True, vmem_limit_bytes=VMEM_BYTES
+        ),
+        name="fused",
+    )(
+        ta, ag[None], wq, wqr, wl, wkr.T, lg[None], wku, wvu, wo, tb, fg[None], ids.T, wts.T,
+        wg, wu, wd, jnp.asarray(near), jnp.asarray(far),
+    )
+
+
+def fused_dims(args):
+    (ta, _, wq, wqr, wl, wkr, _, wku, wvu, wo, tb, _, ids, _, wg, _, wd) = args
+    n, tp = lax.axis_size("ep"), lax.axis_size("tp")
+    experts = wg.shape[0] * n
+    dims = Dims(
+        n=n,
+        cap=2 * tb.shape[0] * ids.shape[1] // experts,
+        rows_a=ta.shape[0],
+        rows_b=tb.shape[0],
+        width=tb.shape[1] // tp,
+        rank=wl.shape[1],
+        heads=wq.shape[1] // NOPE,
+    )
+    copied, buffers = fused_scratch(dims, args)
+    held = sum(math.prod(b.shape) * b.dtype.itemsize for b in copied + buffers)
+    good = (
+        tp == 4
+        and n % 2 == 0
+        and wg.shape[0] == 1
+        and ids.shape[1] == 2
+        and experts <= LANES
+        and dims.cap <= LANES
+        and dims.cap % 16 == 0
+        and held <= VMEM_BYTES * 7 // 8
+    )
+    return dims if good else None
+
+
 def on_device(
     tokens_a,
     attn_gain,
@@ -228,6 +767,13 @@
     w_up,
     w_down,
 ):
+    args = (
+        tokens_a, attn_gain, w_query, w_query_rot, w_latent, w_key_rot, latent_gain, w_key_up,
+        w_value_up, w_output, tokens_b, ffn_gain, expert_ids, expert_weights, w_gate, w_up, w_down,
+    )
+    dims = fused_dims(args)
+    if dims is not None:
+        return fused(dims, args)
     expert_count = w_gate.shape[0] * lax.axis_size("ep")
     outgoing, before = dispatch_rows(tokens_b, ffn_gain, expert_ids, expert_count)
     mixed_a, arrived = attention_half(

time: 172 us -> 91.2 us (0.53)
  Pallas kernels: 0 us -> 87.1 us
  waiting for transfers between devices: 76 us -> 0 us
  matrix products: 43.4 us -> 0 us
  starting transfers between devices: 14.9 us -> 0 us
  between operations: 14.5 us -> 0.65 us
  other arithmetic: 11.3 us -> 0 us
  local copies, waits for them, and re-layouts: 10.7 us -> 3.24 us
    pallas_call x0 -> x1, Pallas kernels: none -> 87.1 us  [fused(): pl.pallas_call(functools.partial(fused_kernel, dims), out_shape=(jax.Shap...]
    all_to_all x2 -> x0, waiting for transfers between devices: 45.6 us -> none  [the longest x1 25.7 us: attention_half(): lax.all_to_all(outgoing, 'ep', split_axis=0, concat_axis=0, tiled=True)]
    dot_general x26 -> x0, matrix products: 43.4 us -> none  [the longest x4 6.69 us: expert_half(): gate_part += jnp.dot(block, gate_rows, preferred_element_type=jnp.float32)]
    all_gather x1 -> x0, waiting for transfers between devices: 14.4 us -> none  [attention_half(): joined = lax.all_gather(compact, 'ep', axis=0, tiled=True)]
    ppermute x6 -> x0, waiting for transfers between devices: 14 us -> none  [swap(): return lax.ppermute(block, 'tp', [(i, i ^ distance) for i in range(count)])]
    all_to_all x2 -> x0, starting transfers between devices: 11 us -> none  [the longest x1 7.31 us: attention_half(): lax.all_to_all(outgoing, 'ep', split_axis=0, concat_axis=0, tiled=True)]
    reshape x2 -> x0, local copies, waits for them, and re-layouts: 7.77 us -> none  [the longest x1 3.89 us: attention_half(): key_blocks = piece_keys.reshape(blocks, row_count, head_count, NOPE)]
    reduce_sum x5 -> x0, other arithmetic: 6.01 us -> none  [the longest x1 3.22 us: attention_half(): block_total = jnp.sum(probs, axis=-1)]
  transfers between devices with their start and end apart: 10 -> 0, of which waited for: 5 -> 0; matrix products, arithmetic and copies ran while one was open for 28% -> 0% of each run, Pallas kernels for 0% -> 0%
where the time goes in v1:
time: 91.2 us; the launch traced here: 91 us
  Pallas kernels  87.1 us (96%)
  local copies, waits for them, and re-layouts  3.24 us (4%)
    pallas_call x1, Pallas kernels, fused(): pl.pallas_call(functools.partial(fused_kernel, dims), out_shape=(jax.Shap...  87.1 us
    unnamed x2, local copies, waits for them, and re-layouts  3.24 us

profile of v1, /device:TPU:0, one launch (start us, length us, event | category | flops | bytes accessed | tf_op | source)
XLA Modules:
  0.0 91.0 jit_solution(12994978126667244782)
XLA Ops:
  0.6 87.1 %fused.1 = (bf16[32,2048]{1,0:T(8,128)(2,1)}, bf16[256,512]{1,0:T(8,128)(2,1)}) custom-call(bf16[128,2048]{1,0:T(8,128)(2,1)} %ta_hbm.1, f32[1,2048]{1,0:T(1,128)} %bitcast.7, bf16[2048,512]{1,0:T(8,128)(2,1)} %wq_hbm.1, bf16[2048,256]{1,0:T(8,128)(2,1)} %wqr_hbm.1, bf16[2048,512]{1,0:T(8,128)(2,1)} %wl_hbm.1, bf16[32,2048]{1,0:T(8,128)(2,1)} %bitcast.6, ...), custom_call_target="tpu_custom_call" | custom-call | tf_op jit(solution)/shard_map/fused/pallas_call | solution.py:704
  87.8 1.6 %copy.23 = bf16[32,2048]{1,0:T(8,128)(2,1)} copy(bf16[32,2048]{1,0:T(8,128)(2,1)} %get-tuple-element.4) | data formatting | bytes 262144
  89.3 1.7 %copy.24 = bf16[256,512]{1,0:T(8,128)(2,1)} copy(bf16[256,512]{1,0:T(8,128)(2,1)} %get-tuple-element.5) | data formatting | bytes 524288

commit v2 on v1

--- a/solution.py
+++ b/solution.py
@@ -218,6 +218,19 @@
     return total.astype(jnp.bfloat16)
 
 
+DOUBLED = (1, 2, 3)
+
+
+SCHEDULES = {
+    8: (
+        "D2", "D1", "enter", "S2", "S1", "D4", "S4", "own", "weights", "E0", "latents", "D5", "S5", "D6", "S6", "P0", "D7", "S7", "D3", "S3", "queries", "tables",
+        "F2", "F1", "R1", "E1", "F4", "R2", "E2", "P1", "U1", "R4", "P2", "E4", "G0", "C0", "F5", "P4", "R5", "blank", "F6", "E5", "G4", "P5", "U2",
+        "G1", "R6", "G2", "F3", "R3", "E6", "G5", "F7", "P6", "E3", "U3", "V0", "V1", "R7", "G6", "E7", "V2", "P7", "P3", "V3",
+        "W", "keys", "A0", "A1", "G7", "A2", "A3", "project", "C1", "C4", "pair", "C5", "G3", "C6", "C2", "C3", "C7",
+    )
+}
+
+
 def rope_tables(rows, blocks):
     half = ROPE // 2
     lane = np.arange(LANES) % ROPE
@@ -230,13 +243,23 @@
     )
 
 
+def staged_as(step):
+    @functools.wraps(step)
+    def run(*given, **options):
+        with jax.named_scope("_".join([step.__name__, *map(str, given)])):
+            return step(*given, **options)
+
+    return run
+
+
 def fused_kernel(
     dims,
-    ta_hbm, ag_ref, wq_hbm, wqr_hbm, wl_hbm, wkr_hbm, lg_ref, wku_hbm, wvu_hbm, wo_hbm,
-    tb_hbm, fg_ref, ids_ref, wts_ref, wg_hbm, wu_hbm, wd_hbm, near_ref, far_ref,
+    ta_hbm, ag_hbm, wq_hbm, wqr_hbm, wl_hbm, wkr_hbm, lg_hbm, wku_hbm, wvu_hbm, wo_hbm,
+    tb_hbm, fg_hbm, ids_hbm, wts_hbm, wg_hbm, wu_hbm, wd_hbm, near_hbm, far_hbm,
     out_a, out_b,
-    ta, wq, wqr, wl, wkr, wku, wvu, wo, tb, wg, wu, wd,
-    own_b, slot_t, slot_c, share_c, staged, landed, part_keep, part_send, part_recv,
+    ta, ag_ref, wq, wqr, wl, wkr, lg_ref, wku, wvu, wo,
+    tb, fg_ref, ids_ref, wts_ref, wg, wu, wd, near_ref, far_ref,
+    own_b, slot_t, slot_c, share_c, staged, wider, landed, part_keep, part_send, part_recv,
     pair_send, pair_recv, back_send, back_recv, total,
     normed_a, rot_w, lat, qs, keys, vals, att, mixed, am_send, am_recv, ax_send, ax_recv,
     load_sem, z_send, z_recv, x_send, x_recv, c_send, c_recv, f_send, f_recv,
@@ -250,13 +273,16 @@
     mate, across = t + 1 - 2 * core, lax.rem(t + 2, 4)
     third = lax.rem(mate + 2, 4)
     quarter = (t, mate, across, third)
+    floors, floor = n // 2, e // 2
     beside = e + 1 - 2 * lax.rem(e, 2)
 
-    def plus(k):
-        return lax.rem(e + k, n)
-
-    def minus(k):
-        return lax.rem(e + n - k, n)
+    def partner(m):
+        there, bit = e, 1
+        while bit < n:
+            if m & bit:
+                there = there + bit - 2 * bit * lax.rem(e // bit, 2)
+            bit *= 2
+        return there
 
     def remote(src, dst, ssem, rsem, ep=None, tp=None):
         target = (e if ep is None else ep, t if tp is None else tp)
@@ -266,18 +292,21 @@
         )
 
     pairs = [
-        (tb_hbm, tb), (ta_hbm, ta), (wl_hbm, wl), (wkr_hbm, wkr), (wg_hbm, wg), (wu_hbm, wu),
-        (wd_hbm, wd), (wq_hbm, wq), (wqr_hbm, wqr), (wku_hbm, wku), (wvu_hbm, wvu), (wo_hbm, wo),
+        (ids_hbm, ids_ref), (tb_hbm, tb), (fg_hbm, fg_ref), (ta_hbm, ta), (ag_hbm, ag_ref),
+        (wl_hbm, wl), (wkr_hbm, wkr), (lg_hbm, lg_ref), (near_hbm, near_ref), (far_hbm, far_ref),
+        (wg_hbm, wg), (wu_hbm, wu), (wd_hbm, wd), (wq_hbm, wq), (wqr_hbm, wqr),
+        (wts_hbm, wts_ref), (wku_hbm, wku), (wvu_hbm, wvu), (wo_hbm, wo),
     ]
     loads = [pltpu.make_async_copy(s, d, load_sem.at[i]) for i, (s, d) in enumerate(pairs)]
     for load in loads:
         load.start()
-    (l_tb, l_ta, l_wl, l_wkr, l_wg, l_wu, l_wd, l_wq, l_wqr, l_wku, l_wvu, l_wo) = loads
+    (l_ids, l_tb, l_fg, l_ta, l_ag, l_wl, l_wkr, l_lg, l_near, l_far) = loads[:10]
+    (l_wg, l_wu, l_wd, l_wq, l_wqr, l_wts, l_wku, l_wvu, l_wo) = loads[10:]
 
     barrier = pltpu.get_barrier_semaphore()
     for k in range(1, n):
         pl.semaphore_signal(
-            barrier, inc=1, device_id=(plus(k), t), device_id_type=pl.DeviceIdType.MESH
+            barrier, inc=1, device_id=(partner(k), t), device_id_type=pl.DeviceIdType.MESH
         )
     for peer in (mate, across):
         pl.semaphore_signal(
@@ -287,39 +316,43 @@
     def own_columns(which):
         return pl.ds(pl.multiple_of(which * width, width), width)
 
-    ids = ids_ref[...]
-    sub = lax.broadcasted_iota(jnp.int32, (LANES, rows_b), 0)
-    first, second = ids[0:1] == sub, ids[1:2] == sub
-    named = jnp.logical_or(first, second)
-    earlier = (
-        lax.broadcasted_iota(jnp.int32, (rows_b, rows_b), 0)
-        < lax.broadcasted_iota(jnp.int32, (rows_b, rows_b), 1)
-    ).astype(jnp.float32).astype(jnp.bfloat16)
-    before = jnp.dot(
-        named.astype(jnp.float32).astype(jnp.bfloat16), earlier, preferred_element_type=jnp.float32
-    )
-    slot = jnp.where(named, before, -1.0)
-    slot_t[...] = slot
-    slot_c[...] = slot.T
-    weight = wts_ref[...]
-    sum_weight = weight[0:1] + weight[1:2]
-    share_c[...] = (
-        jnp.where(first, weight[0:1] / sum_weight, 0.0)
-        + jnp.where(second, weight[1:2] / sum_weight, 0.0)
-    ).T
-
-    l_tb.wait()
-    floats = tb[...].astype(jnp.float32)
-    factor = lax.rsqrt(jnp.mean(floats * floats, axis=-1, keepdims=True) + epsilon)
-    columns = own_columns(t)
-    own_b[...] = (
-        tb[:, columns].astype(jnp.float32) * factor * fg_ref[:, columns]
-    ).astype(jnp.bfloat16)
-
-    pl.semaphore_wait(barrier, n + 1)
+    with jax.named_scope("slots"):
+        l_ids.wait()
+        ids = ids_ref[...]
+        sub = lax.broadcasted_iota(jnp.int32, (LANES, rows_b), 0)
+        first, second = ids[0:1] == sub, ids[1:2] == sub
+        named = jnp.logical_or(first, second)
+        earlier = (
+            lax.broadcasted_iota(jnp.int32, (rows_b, rows_b), 0)
+            < lax.broadcasted_iota(jnp.int32, (rows_b, rows_b), 1)
+        ).astype(jnp.float32).astype(jnp.bfloat16)
+        before = jnp.dot(
+            named.astype(jnp.float32).astype(jnp.bfloat16),
+            earlier,
+            preferred_element_type=jnp.float32,
+        )
+        slot = jnp.where(named, before, -1.0)
+        slot_t[...] = slot
+
+    with jax.named_scope("wait_tb"):
+        l_tb.wait()
+        l_fg.wait()
+    with jax.named_scope("norm_b"):
+        floats = tb[...].astype(jnp.float32)
+        factor = lax.rsqrt(jnp.mean(floats * floats, axis=-1, keepdims=True) + epsilon)
+        for mask in (0, 2):
+            columns = own_columns(quarter[mask])
+            own_b[mask] = (
+                tb[:, columns].astype(jnp.float32) * factor * fg_ref[:, columns]
+            ).astype(jnp.bfloat16)
 
     def z_copy(m):
-        return remote(staged.at[m], landed.at[0, m], z_send.at[m], z_recv.at[m], ep=plus(m))
+        return remote(staged.at[m], landed.at[0, m], z_send.at[m], z_recv.at[m], ep=partner(m))
+
+    def w_copy(m):
+        return remote(
+            wider.at[m], landed.at[2, m], x_send.at[m], x_recv.at[m], ep=partner(m)
+        )
 
     def x_copy(m):
         return remote(landed.at[0, m], landed.at[2, m], x_send.at[m], x_recv.at[m], tp=across)
@@ -337,33 +370,83 @@
         return remote(pair_send.at[m], pair_recv.at[m], q_send.at[m], q_recv.at[m], tp=across)
 
     def b_copy(m):
-        return remote(back_send.at[m], back_recv.at[m], b_send.at[m], b_recv.at[m], ep=minus(m))
-
+        return remote(back_send.at[m], back_recv.at[m], b_send.at[m], b_recv.at[m], ep=partner(m))
+
+    def chosen_for(m):
+        row = slot_t[pl.ds(partner(m), 1), :]
+        wanted = lax.broadcasted_iota(jnp.int32, (cap, rows_b), 0).astype(jnp.float32)
+        return (row == wanted).astype(jnp.float32).astype(jnp.bfloat16)
+
+    @staged_as
     def dispatch(m):
-        row = slot_t[pl.ds(plus(m), 1), :]
-        wanted = lax.broadcasted_iota(jnp.int32, (cap, rows_b), 0).astype(jnp.float32)
-        chosen = (row == wanted).astype(jnp.float32).astype(jnp.bfloat16)
-        picked = jnp.dot(chosen, own_b[...], preferred_element_type=jnp.float32)
+        chosen = chosen_for(m)
+        staged[m] = jnp.dot(chosen, own_b[0], preferred_element_type=jnp.float32).astype(
+            jnp.bfloat16
+        )
+        if m in DOUBLED:
+            wider[m] = jnp.dot(chosen, own_b[2], preferred_element_type=jnp.float32).astype(
+                jnp.bfloat16
+            )
+
+    @staged_as
+    def send(m):
+        z_copy(m).start()
+        if m in DOUBLED:
+            w_copy(m).start()
+
+    @staged_as
+    def enter():
+        pl.semaphore_wait(barrier, n + 1)
+
+    @staged_as
+    def keep_own():
+        floats = tb[...].astype(jnp.float32)
+        factor = lax.rsqrt(jnp.mean(floats * floats, axis=-1, keepdims=True) + epsilon)
+        for mask in (1, 3):
+            columns = own_columns(quarter[mask])
+            own_b[mask] = (
+                tb[:, columns].astype(jnp.float32) * factor * fg_ref[:, columns]
+            ).astype(jnp.bfloat16)
+        chosen = chosen_for(0)
+        for mask in range(4):
+            landed[mask, 0] = jnp.dot(
+                chosen, own_b[mask], preferred_element_type=jnp.float32
+            ).astype(jnp.bfloat16)
+
+    @staged_as
+    def tables():
+        slot_c[...] = slot_t[...].T
+        ids = ids_ref[...]
+        sub = lax.broadcasted_iota(jnp.int32, (LANES, rows_b), 0)
+        l_wts.wait()
+        weight = wts_ref[...]
+        sum_weight = weight[0:1] + weight[1:2]
+        share_c[...] = (
+            jnp.where(ids[0:1] == sub, weight[0:1] / sum_weight, 0.0)
+            + jnp.where(ids[1:2] == sub, weight[1:2] / sum_weight, 0.0)
+        ).T
+
+    @staged_as
+    def forward(m):
+        with jax.named_scope(f"wait_z_copy_{m}"):
+            z_copy(m).wait_recv()
+        if m not in DOUBLED:
+            x_copy(m).start()
+        c_copy(m).start()
+
+    @staged_as
+    def relay(m):
+        with jax.named_scope(f"wait_x_copy_{m}"):
+            (w_copy if m in DOUBLED else x_copy)(m).wait_recv()
+        f_copy(m).start()
+
+    @staged_as
+    def expert(m):
         if m:
-            staged[m] = picked.astype(jnp.bfloat16)
-            z_copy(m).start()
-        else:
-            landed[0, 0] = picked.astype(jnp.bfloat16)
-            x_copy(0).start()
-            c_copy(0).start()
-
-    def forward(m):
-        z_copy(m).wait_recv()
-        x_copy(m).start()
-        c_copy(m).start()
-
-    def relay(m):
-        x_copy(m).wait_recv()
-        f_copy(m).start()
-
-    def expert(m):
-        c_copy(m).wait_recv()
-        f_copy(m).wait_recv()
+            with jax.named_scope(f"wait_c_copy_{m}"):
+                c_copy(m).wait_recv()
+            with jax.named_scope(f"wait_f_copy_{m}"):
+                f_copy(m).wait_recv()
         gate = up = None
         for mask in range(4):
             at = own_columns(quarter[mask])
@@ -382,14 +465,18 @@
                 hidden, wd[0, :, own_columns(quarter[mask])], preferred_element_type=jnp.float32
             )
 
+    @staged_as
     def pair_sum(m):
-        p_copy(m).wait_recv()
+        with jax.named_scope(f"wait_p_copy_{m}"):
+            p_copy(m).wait_recv()
         pair_send[m] = (part_keep[m, 1] + part_recv[m, 1].astype(jnp.float32)).astype(jnp.bfloat16)
         q_copy(m).start()
         part_keep[m, 0] = part_keep[m, 0] + part_recv[m, 0].astype(jnp.float32)
 
+    @staged_as
     def give_back(m):
-        q_copy(m).wait_recv()
+        with jax.named_scope(f"wait_q_copy_{m}"):
+            q_copy(m).wait_recv()
         summed = (part_keep[m, 0] + pair_recv[m].astype(jnp.float32)).astype(jnp.bfloat16)
         if m:
             back_send[m] = summed
@@ -397,10 +484,18 @@
         else:
             back_recv[0] = summed
 
-    def combine(m, begin=False):
+    @staged_as
+    def weights_in():
+        l_wg.wait()
+        l_wu.wait()
+        l_wd.wait()
+
+    @staged_as
+    def combine(m):
         if m:
-            b_copy(m).wait_recv()
-        expert_at = plus(m)
+            with jax.named_scope(f"wait_b_copy_{m}"):
+                b_copy(m).wait_recv()
+        expert_at = partner(m)
         lane = lax.broadcasted_iota(jnp.int32, (rows_b, LANES), 1)
         here = lane == expert_at
         at = jnp.sum(jnp.where(here, slot_c[...], 0.0), axis=1, keepdims=True)
@@ -408,48 +503,56 @@
         wanted = lax.broadcasted_iota(jnp.int32, (rows_b, cap), 1).astype(jnp.float32)
         pick = (at == wanted).astype(jnp.float32).astype(jnp.bfloat16)
         picked = jnp.dot(pick, back_recv[m], preferred_element_type=jnp.float32) * share
-        total[...] = picked if begin else total[...] + picked
+        total[...] = total[...] + picked if m else picked
 
     half_rows = rows_a // 2
     mine = pl.ds(pl.multiple_of(core * half_rows, half_rows), half_rows)
-    quads = n // 2
+    yours = pl.ds(pl.multiple_of((1 - core) * half_rows, half_rows), half_rows)
+
+    def under(k, other=False):
+        return lax.rem((beside if other else e) + n - 2 * k, n)
+
+    def passing(block, ssem, rsem, ep=None, tp=None):
+        return remote(block, block, ssem, rsem, ep, tp)
 
     def lz_copy(k):
-        return remote(
-            lat.at[e, mine], lat.at[e, mine], lz_send.at[k], lz_recv.at[k], ep=plus(2 * k)
+        return passing(
+            lat.at[under(k), mine], lz_send.at[k], lz_recv.at[k + 1], ep=lax.rem(e + 2, n)
         )
 
     def lz_arrival(k):
-        block = lat.at[minus(2 * k), mine]
-        return remote(block, block, lz_send.at[k], lz_recv.at[k], ep=plus(2 * k))
+        return passing(
+            lat.at[under(k), mine], lz_send.at[k], lz_recv.at[k], ep=lax.rem(e + 2, n)
+        )
 
     def ly_copy(k):
-        block = lat.at[minus(2 * k), mine]
-        return remote(block, block, ly_send.at[k], ly_recv.at[k], ep=beside)
+        return passing(lat.at[under(k), mine], ly_send.at[k], ly_recv.at[k], ep=beside)
 
     def ly_arrival(k):
-        block = lat.at[lax.rem(beside + n - 2 * k, n), mine]
-        return remote(block, block, ly_send.at[k], ly_recv.at[k], ep=beside)
-
-    yours = pl.ds(pl.multiple_of((1 - core) * half_rows, half_rows), half_rows)
-
-    def ld_copy(j, owner, part=None):
-        block = lat.at[owner, mine if part is None else part]
-        return remote(block, block, ld_send.at[j], ld_recv.at[j], tp=mate)
-
-    def owner_of(j):
-        return minus(2 * j) if j < quads else lax.rem(beside + n - 2 * (j - quads), n)
-
+        return passing(lat.at[under(k, True), mine], ly_send.at[k], ly_recv.at[k], ep=beside)
+
+    def ld_copy(k, other, rows=None):
+        j = k + floors * other
+        block = lat.at[under(k, other), mine if rows is None else rows]
+        return passing(block, ld_send.at[j], ld_recv.at[j], tp=mate)
+
+    rising = floor < floors - 1
+
+    @staged_as
     def latents():
         l_ta.wait()
+        l_ag.wait()
         rows = ta[...].astype(jnp.float32)
         scale = lax.rsqrt(jnp.mean(rows * rows, axis=-1, keepdims=True) + epsilon)
         normed_a[...] = (rows * scale * ag_ref[...]).astype(jnp.bfloat16)
         l_wl.wait()
+        l_lg.wait()
         raw = jnp.dot(normed_a[...], wl[...], preferred_element_type=jnp.float32)
         scale = lax.rsqrt(jnp.mean(raw * raw, axis=-1, keepdims=True) + epsilon)
         lat[e, :, : dims.rank] = (raw * scale * lg_ref[...]).astype(jnp.bfloat16)
         l_wkr.wait()
+        l_near.wait()
+        l_far.wait()
         plain = wkr[...]
         swapped = jnp.concatenate([-plain[ROPE // 2 :], plain[: ROPE // 2]], axis=0)
         for copy in range(LANES // ROPE):
@@ -462,9 +565,19 @@
         lat[e, :, dims.rank :] = (both[:, :LANES] * cosine + both[:, LANES:] * sine).astype(
             jnp.bfloat16
         )
-        for k in range(1, quads):
-            lz_copy(k).start()
+        pl.when(rising)(lz_copy(0).start)
         ly_copy(0).start()
+
+    @staged_as
+    def blank():
+        for k in range(1, floors):
+
+            @pl.when(floor + k < floors)
+            def _():
+                for side in range(2):
+                    lat[2 * lax.rem(floor + k, floors) + side] = jnp.zeros(
+                        lat.shape[1:], lat.dtype
+                    )
 
     def turn():
         far = far_ref[e]
@@ -472,21 +585,36 @@
         sine = near_ref[1] * far[0:1] + near_ref[0] * far[1:2]
         return cosine, sine
 
-    def latents_on():
-        for k in range(1, quads):
-            lz_arrival(k).wait_recv()
+    @staged_as
+    def latents_on(k):
+        @pl.when(floor >= k)
+        def _():
+            with jax.named_scope("wait_lz"):
+                lz_arrival(k).wait_recv()
+            pl.when(rising)(lz_copy(k).start)
             ly_copy(k).start()
-            ld_copy(k, owner_of(k)).start()
-
-    def latents_over():
-        for k in range(quads):
-            ly_arrival(k).wait_recv()
-            ld_copy(quads + k, owner_of(quads + k)).start()
-
+            ld_copy(k, False).start()
+
+    @staged_as
+    def latents_over(k):
+        @pl.when(floor >= k)
+        def _():
+            with jax.named_scope("wait_ly"):
+                ly_arrival(k).wait_recv()
+            ld_copy(k, True).start()
+
+    @staged_as
     def latents_in():
-        for j in range(1, n):
-            ld_copy(j, owner_of(j), yours).wait_recv()
-
+        for k in range(floors):
+
+            @pl.when(floor >= k)
+            def _():
+                with jax.named_scope("wait_ld"):
+                    if k:
+                        ld_copy(k, False, yours).wait_recv()
+                    ld_copy(k, True, yours).wait_recv()
+
+    @staged_as
     def queries():
         l_wq.wait()
         l_wqr.wait()
@@ -515,6 +643,7 @@
                 qs[p, own, :LANES] = jnp.where(mine_wide, wide, 0.0).astype(jnp.bfloat16)
                 qs[p, own, LANES:] = jnp.where(mine_rot, rot, 0.0).astype(jnp.bfloat16)
 
+    @staged_as
     def key_values():
         l_wku.wait()
         l_wvu.wait()
@@ -528,6 +657,7 @@
 
     logit_scale = (NOPE + ROPE) ** (-0.5)
 
+    @staged_as
     def attend(p):
         at = slice(p * LANES, (p + 1) * LANES)
         contract = (((1,), (1,)), ((), ()))
@@ -560,6 +690,7 @@
     am_copy = remote(am_send, am_recv, as_send, as_recv, tp=mate)
     ax_copy = remote(ax_send, ax_recv, at_send, at_recv, tp=across)
 
+    @staged_as
     def project():
         l_wo.wait()
         mixed[...] = jnp.dot(att[...], wo[...], preferred_element_type=jnp.float32).astype(
@@ -569,68 +700,55 @@
             am_send[place] = mixed[rows_of(quarter[mask]), :].astype(jnp.bfloat16)
         am_copy.start()
 
+    @staged_as
     def project_pair():
-        am_copy.wait_recv()
+        with jax.named_scope(f"wait_am_copy"):
+            am_copy.wait_recv()
         ax_send[...] = (mixed[rows_of(across), :] + am_recv[1].astype(jnp.float32)).astype(
             jnp.bfloat16
         )
         ax_copy.start()
 
+    @staged_as
     def project_end():
-        ax_copy.wait_recv()
+        with jax.named_scope(f"wait_ax_copy"):
+            ax_copy.wait_recv()
         out_a[...] = (
             mixed[rows_of(t), :]
             + am_recv[0].astype(jnp.float32)
             + ax_recv[...].astype(jnp.float32)
         ).astype(jnp.bfloat16)
 
-    dispatch(1)
-    dispatch(0)
-    for m in range(2, n):
-        dispatch(m)
-    latents()
-    l_wg.wait()
-    l_wu.wait()
-    l_wd.wait()
-    order = list(range(1, n)) + [0]
-    pairs_of_heads = dims.heads // 2
-    extra = {0: [queries], 1: [latents_on], 2: [latents_over], 3: [latents_in, key_values]}
-    for p in range(pairs_of_heads):
-        extra.setdefault(4 + p, []).append(functools.partial(attend, p))
-    extra.setdefault(4 + pairs_of_heads, []).append(project)
-    extra.setdefault(5 + pairs_of_heads, []).append(project_pair)
-    for i in range(max(n + 4, 6 + pairs_of_heads)):
-        if i < n - 1:
-            forward(order[i])
-        if i == 0:
-            relay(0)
-        elif i <= n - 1:
-            relay(order[i - 1])
-        if 2 <= i < n + 2:
-            expert(order[i - 2])
-        if 3 <= i < n + 3:
-            pair_sum(order[i - 3])
-        if 4 <= i < n + 4:
-            give_back(order[i - 4])
-        for step in extra.get(i, []):
-            step()
-    for i, m in enumerate(order):
-        combine(m, begin=i == 0)
+    stages = dict(
+        D=dispatch, S=send, enter=enter, F=forward, R=relay, E=expert, P=pair_sum, G=give_back, C=combine,
+        latents=latents, own=keep_own, queries=queries, tables=tables, blank=blank,
+        U=latents_on, V=latents_over, W=latents_in, keys=key_values, A=attend,
+        project=project, pair=project_pair, weights=weights_in,
+    )
+    for entry in SCHEDULES[n]:
+        if entry in stages:
+            stages[entry]()
+        else:
+            stages[entry[0]](int(entry[1:]))
     out_b[...] = total[...].astype(jnp.bfloat16)
     project_end()
 
+    for m in range(1, n):
+        for make in (z_copy, c_copy, f_copy, b_copy, w_copy if m in DOUBLED else x_copy):
+            make(m).wait_send()
     for m in range(n):
-        if m:
-            z_copy(m).wait_send()
-            b_copy(m).wait_send()
-        for make in (x_copy, c_copy, f_copy, p_copy, q_copy):
-            make(m).wait_send()
-    for k in range(quads):
-        if k:
-            lz_copy(k).wait_send()
-        ly_copy(k).wait_send()
-    for j in range(1, n):
-        ld_copy(j, owner_of(j)).wait_send()
+        p_copy(m).wait_send()
+        q_copy(m).wait_send()
+    for k in range(floors):
+
+        @pl.when(floor >= k)
+        def _():
+            pl.when(rising)(lz_copy(k).wait_send)
+            ly_copy(k).wait_send()
+            if k:
+                ld_copy(k, False).wait_send()
+            ld_copy(k, True).wait_send()
+
     am_copy.wait_send()
     ax_copy.wait_send()
 
@@ -647,21 +765,20 @@
 
 
 def fused_scratch(dims, args):
-    (ta, _, wq, wqr, wl, wkr, _, wku, wvu, wo, tb, _, _, _, wg, wu, wd) = args
+    ta, wku, wvu = args[0], args[7], args[8]
     n, cap, width, rows_a, rows_b = dims.n, dims.cap, dims.width, dims.rows_a, dims.rows_b
     model = ta.shape[1]
     bf, f32 = jnp.bfloat16, jnp.float32
     vmem = pltpu.VMEM
-    copied = [vmem(a.shape, a.dtype) for a in (ta, wq, wqr, wl)]
-    copied.append(vmem((wkr.shape[1], wkr.shape[0]), wkr.dtype))
-    copied += [vmem(a.shape, a.dtype) for a in (wku, wvu, wo, tb, wg, wu, wd)]
+    copied = [vmem(a.shape, a.dtype) for a in args]
     block = (cap, width)
     quarter_rows = rows_a // 4
     return copied, [
-        vmem((rows_b, width), bf),
+        vmem((4, rows_b, width), bf),
         vmem((LANES, rows_b), f32),
         vmem((rows_b, LANES), f32),
         vmem((rows_b, LANES), f32),
+        vmem((n, *block), bf),
         vmem((n, *block), bf),
         vmem((4, n, *block), bf),
         vmem((n, 2, *block), f32),
@@ -688,33 +805,34 @@
 
 
 def fused(dims, args):
-    (ta, ag, wq, wqr, wl, wkr, lg, wku, wvu, wo, tb, fg, ids, wts, wg, wu, wd) = args
+    ta = args[0]
+    args = fused_operands(dims, args)
     copied, buffers = fused_scratch(dims, args)
     n = dims.n
     dma = pltpu.SemaphoreType.DMA
     sems = [dma((len(copied),))] + [dma((n,)) for _ in range(14)]
-    sems += [dma((n,)) for _ in range(6)] + [dma, dma, dma, dma]
-    near, far = rope_tables(dims.rows_a, n)
-    anywhere = pl.BlockSpec(memory_space=pl.ANY)
+    sems += [dma((n + 1,)) for _ in range(6)] + [dma, dma, dma, dma]
     inside = pl.BlockSpec(memory_space=pltpu.VMEM)
-    where = [
-        anywhere, inside, anywhere, anywhere, anywhere, anywhere, inside, anywhere, anywhere,
-        anywhere, anywhere, inside, inside, inside, anywhere, anywhere, anywhere, inside, inside,
-    ]
     return pl.pallas_call(
         functools.partial(fused_kernel, dims),
         out_shape=(
-            jax.ShapeDtypeStruct((dims.rows_a // 4, ta.shape[1]), jnp.bfloat16),
-            jax.ShapeDtypeStruct((dims.rows_b, dims.width), jnp.bfloat16),
+            pltpu.VMEM((dims.rows_a // 4, ta.shape[1]), jnp.bfloat16),
+            pltpu.VMEM((dims.rows_b, dims.width), jnp.bfloat16),
         ),
-        in_specs=where,
+        in_specs=[pl.BlockSpec(memory_space=pltpu.HBM)] * len(args),
         out_specs=(inside, inside),
         scratch_shapes=copied + buffers + sems,
         compiler_params=pltpu.CompilerParams(
             collective_id=0, has_side_effects=True, vmem_limit_bytes=VMEM_BYTES
         ),
         name="fused",
-    )(
+    )(*args)
+
+
+def fused_operands(dims, args):
+    (ta, ag, wq, wqr, wl, wkr, lg, wku, wvu, wo, tb, fg, ids, wts, wg, wu, wd) = args
+    near, far = rope_tables(dims.rows_a, dims.n)
+    return (
         ta, ag[None], wq, wqr, wl, wkr.T, lg[None], wku, wvu, wo, tb, fg[None], ids.T, wts.T,
         wg, wu, wd, jnp.asarray(near), jnp.asarray(far),
     )
@@ -736,14 +854,16 @@
     copied, buffers = fused_scratch(dims, args)
     held = sum(math.prod(b.shape) * b.dtype.itemsize for b in copied + buffers)
     good = (
-        tp == 4
-        and n % 2 == 0
+        n in SCHEDULES
+        and tp == 4
+        and n & (n - 1) == 0
+        and dims.heads == 8
         and wg.shape[0] == 1
         and ids.shape[1] == 2
         and experts <= LANES
         and dims.cap <= LANES
         and dims.cap % 16 == 0
-        and held <= VMEM_BYTES * 7 // 8
+        and held <= VMEM_BYTES
     )
     return dims if good else None
 

time: 91.2 us -> 67.3 us (0.74)
  Pallas kernels: 87.1 us -> 65.1 us
  local copies, waits for them, and re-layouts: 3.24 us -> 1.36 us
    pallas_call x1, Pallas kernels: 87.1 us -> 65.1 us  [fused(): pl.pallas_call(functools.partial(fused_kernel, dims), out_shape=(pltpu.VM...]
    unnamed x2, local copies, waits for them, and re-layouts: 3.24 us -> 1.36 us
where the time goes in v2:
time: 67.3 us; the launch traced here: 67.1 us
  Pallas kernels  65.1 us (97%)
  local copies, waits for them, and re-layouts  1.36 us (2%)
    pallas_call x1, Pallas kernels, fused(): pl.pallas_call(functools.partial(fused_kernel, dims), out_shape=(pltpu.VM...  65.1 us
    unnamed x2, local copies, waits for them, and re-layouts  1.36 us

profile of v2, /device:TPU:0, one launch (start us, length us, event | category | flops | bytes accessed | tf_op | source)
XLA Modules:
  0.0 67.1 jit_solution(1094817250230943374)
XLA Ops:
  0.6 65.1 %fused.1 = (bf16[32,2048]{1,0:T(8,128)(2,1)S(1)}, bf16[256,512]{1,0:T(8,128)(2,1)S(1)}) custom-call(bf16[128,2048]{1,0:T(8,128)(2,1)} %ta_hbm.1, f32[1,2048]{1,0:T(1,128)} %bitcast.7, bf16[2048,512]{1,0:T(8,128)(2,1)} %wq_hbm.1, bf16[2048,256]{1,0:T(8,128)(2,1)} %wqr_hbm.1, bf16[2048,512]{1,0:T(8,128)(2,1)} %wl_hbm.1, bf16[32,2048]{1,0:T(8,128)(2,1)} %bitcast.6, ...), custom_call_target="tpu_custom_call" | custom-call | tf_op jit(solution)/shard_map/fused/pallas_call | solution.py:816
  65.7 0.7 copy.23
  66.4 0.7 %copy.24 = bf16[256,512]{1,0:T(8,128)(2,1)} copy(bf16[256,512]{1,0:T(8,128)(2,1)S(1)} %get-tuple-element.3) | data formatting | bytes 524288

commit v3 on v2

--- a/solution.py
+++ b/solution.py
@@ -219,14 +219,15 @@
 
 
 DOUBLED = (1, 2, 3)
+UNMIXED = (0, 1, 2)
 
 
 SCHEDULES = {
     8: (
-        "D2", "D1", "enter", "S2", "S1", "D4", "S4", "own", "weights", "E0", "latents", "D5", "S5", "D6", "S6", "P0", "D7", "S7", "D3", "S3", "queries", "tables",
-        "F2", "F1", "R1", "E1", "F4", "R2", "E2", "P1", "U1", "R4", "P2", "E4", "G0", "C0", "F5", "P4", "R5", "blank", "F6", "E5", "G4", "P5", "U2",
-        "G1", "R6", "G2", "F3", "R3", "E6", "G5", "F7", "P6", "E3", "U3", "V0", "V1", "R7", "G6", "E7", "V2", "P7", "P3", "V3",
-        "W", "keys", "A0", "A1", "G7", "A2", "A3", "project", "C1", "C4", "pair", "C5", "G3", "C6", "C2", "C3", "C7",
+        "D2", "enter", "S2", "D1", "S1", "D4", "S4", "own", "weights", "E0", "latents", "D5", "S5", "D6", "S6", "P0", "D3", "S3", "queries", "tables",
+        "F2", "F1", "R1", "E1", "F4", "R2", "E2", "P1", "U1", "D7", "S7", "P2", "R4", "C0", "E4", "F5", "P4", "F6", "blank", "R5", "E5", "G4", "P5", "F7", "U2",
+        "R6", "F3", "R3", "E6", "G5", "E3", "P6", "C1", "U3", "V0", "V1", "P3", "R7", "V2", "E7", "C2", "G6", "V3", "P7", "N",
+        "W", "keys", "G3", "A0", "A1", "G7", "A2", "A3", "project", "C4", "C5", "pair", "C6", "C3", "C7", "M",
     )
 }
 
@@ -260,10 +261,10 @@
     ta, ag_ref, wq, wqr, wl, wkr, lg_ref, wku, wvu, wo,
     tb, fg_ref, ids_ref, wts_ref, wg, wu, wd, near_ref, far_ref,
     own_b, slot_t, slot_c, share_c, staged, wider, landed, part_keep, part_send, part_recv,
-    pair_send, pair_recv, back_send, back_recv, total,
+    pair_send, pair_recv, back_send, back_recv, side_send, side_recv, total, total_side, near_send, near_recv,
     normed_a, rot_w, lat, qs, keys, vals, att, mixed, am_send, am_recv, ax_send, ax_recv,
     load_sem, z_send, z_recv, x_send, x_recv, c_send, c_recv, f_send, f_recv,
-    p_send, p_recv, q_send, q_recv, b_send, b_recv,
+    p_send, p_recv, q_send, q_recv, b_send, b_recv, s_send, s_recv, n_send, n_recv,
     lz_send, lz_recv, ly_send, ly_recv, ld_send, ld_recv, as_send, as_recv, at_send, at_recv,
 ):
     n, cap, rows_a, rows_b = dims.n, dims.cap, dims.rows_a, dims.rows_b
@@ -371,6 +372,11 @@
 
     def b_copy(m):
         return remote(back_send.at[m], back_recv.at[m], b_send.at[m], b_recv.at[m], ep=partner(m))
+
+    def s_copy(m):
+        return remote(
+            side_send.at[m], side_recv.at[m], s_send.at[m], s_recv.at[m], ep=partner(m)
+        )
 
     def chosen_for(m):
         row = slot_t[pl.ds(partner(m), 1), :]
@@ -469,7 +475,19 @@
     def pair_sum(m):
         with jax.named_scope(f"wait_p_copy_{m}"):
             p_copy(m).wait_recv()
-        pair_send[m] = (part_keep[m, 1] + part_recv[m, 1].astype(jnp.float32)).astype(jnp.bfloat16)
+        side = (part_keep[m, 1] + part_recv[m, 1].astype(jnp.float32)).astype(jnp.bfloat16)
+        if m in UNMIXED:
+            own = (part_keep[m, 0] + part_recv[m, 0].astype(jnp.float32)).astype(jnp.bfloat16)
+            if m:
+                back_send[m] = own
+                b_copy(m).start()
+                side_send[m] = side
+                s_copy(m).start()
+            else:
+                back_recv[0] = own
+                side_recv[0] = side
+            return
+        pair_send[m] = side
         q_copy(m).start()
         part_keep[m, 0] = part_keep[m, 0] + part_recv[m, 0].astype(jnp.float32)
 
@@ -504,6 +522,25 @@
         pick = (at == wanted).astype(jnp.float32).astype(jnp.bfloat16)
         picked = jnp.dot(pick, back_recv[m], preferred_element_type=jnp.float32) * share
         total[...] = total[...] + picked if m else picked
+        if m in UNMIXED:
+            if m:
+                with jax.named_scope(f"wait_s_copy_{m}"):
+                    s_copy(m).wait_recv()
+            picked = jnp.dot(pick, side_recv[m], preferred_element_type=jnp.float32) * share
+            total_side[...] = total_side[...] + picked if m else picked
+
+    n_copy = remote(near_send, near_recv, n_send, n_recv, tp=across)
+
+    @staged_as
+    def near_out():
+        near_send[...] = total_side[...].astype(jnp.bfloat16)
+        n_copy.start()
+
+    @staged_as
+    def near_in():
+        with jax.named_scope("wait_n_copy"):
+            n_copy.wait_recv()
+        total[...] = total[...] + near_recv[...].astype(jnp.float32)
 
     half_rows = rows_a // 2
     mine = pl.ds(pl.multiple_of(core * half_rows, half_rows), half_rows)
@@ -518,6 +555,11 @@
     def lz_copy(k):
         return passing(
             lat.at[under(k), mine], lz_send.at[k], lz_recv.at[k + 1], ep=lax.rem(e + 2, n)
+        )
+
+    def lz_far():
+        return passing(
+            lat.at[under(1), mine], lz_send.at[2], lz_recv.at[3], ep=lax.rem(e + 4, n)
         )
 
     def lz_arrival(k):
@@ -537,6 +579,7 @@
         return passing(block, ld_send.at[j], ld_recv.at[j], tp=mate)
 
     rising = floor < floors - 1
+    rising_far = floor < floors - 2
 
     @staged_as
     def latents():
@@ -591,7 +634,9 @@
         def _():
             with jax.named_scope("wait_lz"):
                 lz_arrival(k).wait_recv()
-            pl.when(rising)(lz_copy(k).start)
+            if k == 1:
+                pl.when(rising)(lz_copy(1).start)
+                pl.when(rising_far)(lz_far().start)
             ly_copy(k).start()
             ld_copy(k, False).start()
 
@@ -723,7 +768,7 @@
         D=dispatch, S=send, enter=enter, F=forward, R=relay, E=expert, P=pair_sum, G=give_back, C=combine,
         latents=latents, own=keep_own, queries=queries, tables=tables, blank=blank,
         U=latents_on, V=latents_over, W=latents_in, keys=key_values, A=attend,
-        project=project, pair=project_pair, weights=weights_in,
+        N=near_out, M=near_in, project=project, pair=project_pair, weights=weights_in,
     )
     for entry in SCHEDULES[n]:
         if entry in stages:
@@ -738,12 +783,19 @@
             make(m).wait_send()
     for m in range(n):
         p_copy(m).wait_send()
-        q_copy(m).wait_send()
+        if m not in UNMIXED:
+            q_copy(m).wait_send()
+        elif m:
+            s_copy(m).wait_send()
+    n_copy.wait_send()
     for k in range(floors):
 
         @pl.when(floor >= k)
         def _():
-            pl.when(rising)(lz_copy(k).wait_send)
+            if k <= 1:
+                pl.when(rising)(lz_copy(k).wait_send)
+            if k == 1:
+                pl.when(rising_far)(lz_far().wait_send)
             ly_copy(k).wait_send()
             if k:
                 ld_copy(k, False).wait_send()
@@ -788,7 +840,12 @@
         vmem((n, *block), bf),
         vmem((n, *block), bf),
         vmem((n, *block), bf),
+        vmem((n // 2, *block), bf),
+        vmem((n // 2, *block), bf),
         vmem((rows_b, width), f32),
+        vmem((rows_b, width), f32),
+        vmem((rows_b, width), bf),
+        vmem((rows_b, width), bf),
         vmem((rows_a, model), bf),
         vmem((2 * LANES, model), bf),
         vmem((n, rows_a, dims.rank + LANES), bf),
@@ -810,7 +867,7 @@
     copied, buffers = fused_scratch(dims, args)
     n = dims.n
     dma = pltpu.SemaphoreType.DMA
-    sems = [dma((len(copied),))] + [dma((n,)) for _ in range(14)]
+    sems = [dma((len(copied),))] + [dma((n,)) for _ in range(16)] + [dma, dma]
     sems += [dma((n + 1,)) for _ in range(6)] + [dma, dma, dma, dma]
     inside = pl.BlockSpec(memory_space=pltpu.VMEM)
     return pl.pallas_call(

time: 67.3 us -> 61.9 us (0.920)
  Pallas kernels: 65.1 us -> 59.8 us
    pallas_call x1, Pallas kernels: 65.1 us -> 59.8 us  [fused(): pl.pallas_call(functools.partial(fused_kernel, dims), out_shape=(pltpu.VM...]
where the time goes in v3:
time: 61.9 us; the launch traced here: 61.8 us
  Pallas kernels  59.8 us (97%)
  local copies, waits for them, and re-layouts  1.36 us (2%)
  between operations  0.65 us (1%)
    pallas_call x1, Pallas kernels, fused(): pl.pallas_call(functools.partial(fused_kernel, dims), out_shape=(pltpu.VM...  59.8 us
    unnamed x2, local copies, waits for them, and re-layouts  1.36 us

profile of v3, /device:TPU:0, one launch (start us, length us, event | category | flops | bytes accessed | tf_op | source)
XLA Modules:
  0.0 61.8 jit_solution(5066717046983236492)
XLA Ops:
  0.6 59.8 %fused.1 = (bf16[32,2048]{1,0:T(8,128)(2,1)S(1)}, bf16[256,512]{1,0:T(8,128)(2,1)S(1)}) custom-call(bf16[128,2048]{1,0:T(8,128)(2,1)} %ta_hbm.1, f32[1,2048]{1,0:T(1,128)} %bitcast.7, bf16[2048,512]{1,0:T(8,128)(2,1)} %wq_hbm.1, bf16[2048,256]{1,0:T(8,128)(2,1)} %wqr_hbm.1, bf16[2048,512]{1,0:T(8,128)(2,1)} %wl_hbm.1, bf16[32,2048]{1,0:T(8,128)(2,1)} %bitcast.6, ...), custom_call_target="tpu_custom_call" | custom-call | tf_op jit(solution)/shard_map/fused/pallas_call | solution.py:873
  60.4 0.7 %copy.23 = bf16[32,2048]{1,0:T(8,128)(2,1)} copy(bf16[32,2048]{1,0:T(8,128)(2,1)S(1)} %get-tuple-element.2) | data formatting | bytes 262144
  61.1 0.7 %copy.24 = bf16[256,512]{1,0:T(8,128)(2,1)} copy(bf16[256,512]{1,0:T(8,128)(2,1)S(1)} %get-tuple-element.3) | data formatting | bytes 524288

commit v4 on v3

--- a/solution.py
+++ b/solution.py
@@ -225,9 +225,9 @@
 SCHEDULES = {
     8: (
         "D2", "enter", "S2", "D1", "S1", "D4", "S4", "own", "weights", "E0", "latents", "D5", "S5", "D6", "S6", "P0", "D3", "S3", "queries", "tables",
-        "F2", "F1", "R1", "E1", "F4", "R2", "E2", "P1", "U1", "D7", "S7", "P2", "R4", "C0", "E4", "F5", "P4", "F6", "blank", "R5", "E5", "G4", "P5", "F7", "U2",
-        "R6", "F3", "R3", "E6", "G5", "E3", "P6", "C1", "U3", "V0", "V1", "P3", "R7", "V2", "E7", "C2", "G6", "V3", "P7", "N",
-        "W", "keys", "G3", "A0", "A1", "G7", "A2", "A3", "project", "C4", "C5", "pair", "C6", "C3", "C7", "M",
+        "F2", "F1", "R1", "E1", "F4", "R2", "E2", "U1", "D7", "S7", "R4", "P1", "E4", "F5", "P2", "P4", "F6", "C0", "blank", "R5", "E5", "G4", "P5", "F7", "U2",
+        "R6", "F3", "R3", "E6", "G5", "E3", "P6", "U3", "C1", "V0", "V1", "R7", "P3", "V2", "E7", "C2", "P7", "V3", "G6", "N",
+        "W", "keys", "G3", "A0", "A1", "G7", "A2", "A3", "project", "C4", "C5", "pair", "C6", "C7", "C3", "M",
     )
 }
 

time: 61.9 us -> 61.8 us (level)
  no operation moved by 1% of the time
where the time goes in v4:
time: 61.8 us; the launch traced here: 61.6 us
  Pallas kernels  59.6 us (96%)
  local copies, waits for them, and re-layouts  1.36 us (2%)
  between operations  0.65 us (1%)
    pallas_call x1, Pallas kernels, fused(): pl.pallas_call(functools.partial(fused_kernel, dims), out_shape=(pltpu.VM...  59.6 us
    unnamed x2, local copies, waits for them, and re-layouts  1.36 us

profile of v4, /device:TPU:0, one launch (start us, length us, event | category | flops | bytes accessed | tf_op | source)
XLA Modules:
  0.0 61.6 jit_solution(13522964581676776639)
XLA Ops:
  0.6 59.6 %fused.1 = (bf16[32,2048]{1,0:T(8,128)(2,1)S(1)}, bf16[256,512]{1,0:T(8,128)(2,1)S(1)}) custom-call(bf16[128,2048]{1,0:T(8,128)(2,1)} %ta_hbm.1, f32[1,2048]{1,0:T(1,128)} %bitcast.7, bf16[2048,512]{1,0:T(8,128)(2,1)} %wq_hbm.1, bf16[2048,256]{1,0:T(8,128)(2,1)} %wqr_hbm.1, bf16[2048,512]{1,0:T(8,128)(2,1)} %wl_hbm.1, bf16[32,2048]{1,0:T(8,128)(2,1)} %bitcast.6, ...), custom_call_target="tpu_custom_call" | custom-call | tf_op jit(solution)/shard_map/fused/pallas_call | solution.py:873
  60.3 0.7 %copy.23 = bf16[32,2048]{1,0:T(8,128)(2,1)} copy(bf16[32,2048]{1,0:T(8,128)(2,1)S(1)} %get-tuple-element.2) | data formatting | bytes 262144
  60.9 0.7 %copy.24 = bf16[256,512]{1,0:T(8,128)(2,1)} copy(bf16[256,512]{1,0:T(8,128)(2,1)S(1)} %get-tuple-element.3) | data formatting | bytes 524288
